TPU v7x, 32 devices: a whole 2x2x4 slice. The times are simulated.
32 devices in a mesh: sp: 8 (over z, x), tp: 4 (over y, core).
Axes of the slice: x: 2, y: 2, z: 4, core: 2. Of those that a mesh axis runs over, the one named last changes fastest.
Arguments:
- queries: bfloat16 [1024, 2048], P('sp', 'tp'), may hold values from -6 to 6
- key_rows: bfloat16 [1024, 2048], P('sp', 'tp'), may hold values from -6 to 6
- value_rows: bfloat16 [1024, 2048], P('sp', 'tp'), may hold values from -6 to 6
- gate_input: bfloat16 [1024, 2048], P('sp', 'tp'), may hold values from -6 to 6
- log_decay: float32 [1024, 16], P('sp', 'tp'), may hold values from -0.6 to 0, as said below
- head_gain: float32 [2048], P('tp'), may hold values from 0.1 to 1.9
- out_weight: bfloat16 [2048, 2048], P('tp'), may hold values from -0.125 to 0.125
- residual: bfloat16 [1024, 2048], P('sp'), may hold values from -6 to 6
- mlp_gain: float32 [2048], replicated, may hold values from 0.1 to 1.9
- gate_weight: bfloat16 [2048, 5632], P('sp', 'tp'), may hold values from -0.125 to 0.125
- up_weight: bfloat16 [2048, 5632], P('sp', 'tp'), may hold values from -0.125 to 0.125
- down_weight: bfloat16 [5632, 2048], P('tp', 'sp'), may hold values from -0.078125 to 0.078125
Outputs:
- layer_out: bfloat16 [1024, 2048], P(('sp', 'tp'))
Inputs may be any that keep to these rules, and one draw needn't show every extreme that they name: log_decay holds the logarithm of a decay factor of each head at each position.
All inputs are finite; a program needn't handle non-finite values.
Results may differ from a plain program's by a relative error of at most 0.017.
Values may be sent and summed in bfloat16 or wider, within the bound.
A program may use at most 128 MiB of HBM per device.

v0:
```python
import functools
import math

import jax
import jax.numpy as jnp
from jax import lax
from jax.experimental import pallas as pl
from jax.experimental.pallas import tpu as pltpu
from jax.sharding import PartitionSpec as P

BLOCK = 128


EPS = 1e-06


def prefix_2(x, axis, join, neutral):
    place = lax.axis_index(axis)
    gathered = jax.tree.map(
        lambda a, kind: lax.all_gather(a.astype(kind), axis), x, (jnp.bfloat16, jnp.bfloat16)
    )
    state = jax.tree.map(lambda a, e: jnp.zeros_like(a) + jnp.asarray(e, a.dtype), x, neutral)

    def one(step, state):
        return join(
            state,
            jax.tree.map(
                lambda a, own: lax.dynamic_index_in_dim(a, step, 0, False).astype(own.dtype),
                gathered,
                x,
            ),
        )

    return lax.fori_loop(0, place, one, state)


def rotate(values_in, positions):
    half = values_in.shape[-1] // 2
    freq = 10000.0 ** (-jnp.linspace(0.0, 1.0, half, dtype=jnp.float32))
    angles = positions * freq
    angles = jnp.concatenate([angles, angles], axis=-1)
    first = values_in[..., :half]
    second = values_in[..., half:]
    turned = jnp.concatenate([-second, first], axis=-1)
    return values_in * jnp.cos(angles) + turned * jnp.sin(angles)


def row_norm(stream, gain):
    return stream * lax.rsqrt(jnp.mean(stream * stream, axis=-1, keepdims=True) + EPS) * gain


def join_states(earlier, later):
    return (earlier[0] * later[0], later[0][:, None, None] * earlier[1] + later[1])


def body(
    queries,
    key_rows,
    value_rows,
    gate_input,
    log_decay,
    head_gain,
    out_weight,
    residual,
    mlp_gain,
    gate_weight,
    up_weight,
    down_weight,
):
    tok_rows = queries.shape[0]
    heads_here = log_decay.shape[1]
    head_size = head_gain.shape[0] // heads_here
    quarter = tok_rows // lax.axis_size("tp")
    offset = lax.axis_index("sp") * tok_rows
    positions = (offset + lax.iota(jnp.int32, tok_rows)).astype(jnp.float32)[:, None, None]
    q_rot = rotate(
        queries.reshape(tok_rows, heads_here, head_size).astype(jnp.float32), positions
    ).astype(jnp.bfloat16)
    k_rot = (
        rotate(key_rows.reshape(tok_rows, heads_here, head_size).astype(jnp.float32), positions)
        * head_size ** (-0.5)
    ).astype(jnp.bfloat16)
    blocks = tok_rows // BLOCK
    q_blocks = q_rot.reshape(blocks, BLOCK, heads_here, head_size)
    k_blocks = k_rot.reshape(blocks, BLOCK, heads_here, head_size)
    v_blocks = value_rows.reshape(blocks, BLOCK, heads_here, head_size)
    cumul = jnp.cumsum(log_decay.reshape(blocks, BLOCK, heads_here), axis=1)
    by_head = cumul.transpose(0, 2, 1)
    lower = jnp.tril(jnp.ones((BLOCK, BLOCK), dtype=bool))
    spread = by_head[:, :, :, None] - by_head[:, :, None, :]
    weight = jnp.where(lower, jnp.exp(jnp.where(lower, spread, 0.0)), 0.0)
    scores = jnp.einsum("nthd,nshd->nhts", q_blocks, k_blocks, preferred_element_type=jnp.float32)
    probs = (scores * weight).astype(jnp.bfloat16)
    inner = jnp.einsum("nhts,nshe->nthe", probs, v_blocks, preferred_element_type=jnp.float32)
    k_weighted = (
        k_blocks.astype(jnp.float32) * jnp.exp(cumul[:, -1:, :] - cumul)[..., None]
    ).astype(jnp.bfloat16)
    contrib = jnp.einsum(
        "nshd,nshe->nhde", k_weighted, v_blocks, preferred_element_type=jnp.float32
    )
    totals = jnp.exp(cumul[:, -1, :])

    def advance(carry, items):
        state, prefix = carry
        factor, update = items
        return ((state * factor[:, None, None] + update, prefix * factor), (state, prefix))

    start_state = jnp.zeros((heads_here, head_size, head_size), jnp.float32)
    start_prefix = jnp.ones((heads_here,), jnp.float32)
    (dev_state, dev_total), (local_before, prefixes) = lax.scan(
        advance, (start_state, start_prefix), (totals, contrib)
    )
    _, incoming = prefix_2((dev_total, dev_state), "sp", join_states, (start_prefix, start_state))
    before = local_before + prefixes[:, :, None, None] * incoming[None]
    cross = jnp.einsum(
        "nthd,nhde->nthe", q_blocks.astype(jnp.float32), before, precision=lax.Precision.HIGHEST
    )
    cross = cross * jnp.exp(cumul)[..., None]
    result = (inner + cross).reshape(tok_rows, heads_here, head_size)
    result = row_norm(result, head_gain.reshape(heads_here, head_size)).reshape(
        tok_rows, heads_here * head_size
    )
    retained = (result * jax.nn.silu(gate_input.astype(jnp.float32))).astype(jnp.bfloat16)
    picked = retained
    mixed = lax.psum_scatter(
        jnp.dot(picked, out_weight, preferred_element_type=jnp.float32).astype(jnp.bfloat16),
        "tp",
        scatter_dimension=0,
        tiled=True,
    ).astype(jnp.float32)
    own_rows = lax.dynamic_slice_in_dim(residual, lax.axis_index("tp") * quarter, quarter, 0)
    rows_mid = (own_rows.astype(jnp.float32) + mixed).astype(jnp.bfloat16)
    own_normed = row_norm(rows_mid.astype(jnp.float32), mlp_gain).astype(jnp.bfloat16)
    normed = lax.all_gather(own_normed, "tp", axis=0, tiled=True)
    gate = jnp.dot(
        normed,
        lax.all_gather(gate_weight, "sp", axis=0, tiled=True),
        preferred_element_type=jnp.float32,
    )
    upvals = jnp.dot(
        normed,
        lax.all_gather(up_weight, "sp", axis=0, tiled=True),
        preferred_element_type=jnp.float32,
    )
    full_down = lax.all_gather(down_weight, "sp", axis=1, tiled=True)
    hidden = (jax.nn.silu(gate) * upvals).astype(jnp.bfloat16)
    picked = hidden
    ffn = lax.psum_scatter(
        jnp.dot(picked, full_down, preferred_element_type=jnp.float32).astype(jnp.bfloat16),
        "tp",
        scatter_dimension=0,
        tiled=True,
    ).astype(jnp.float32)
    return (rows_mid.astype(jnp.float32) + ffn).astype(jnp.bfloat16)


MESH = pl.DeviceIdType.MESH
XS = 2
CS = 2
F32 = jnp.float32
BF16 = jnp.bfloat16


def dot_nt(a, b):
    return lax.dot_general(a, b, (((1,), (1,)), ((), ())), preferred_element_type=F32)


def dot_nn(a, b):
    return lax.dot_general(a, b, (((1,), (0,)), ((), ())), preferred_element_type=F32)


def kernel(
    nz,
    nt,
    q_ref,
    k_ref,
    v_ref,
    g_ref,
    ld_ref,
    hg_ref,
    res_ref,
    mg_ref,
    ow_hbm,
    gw_hbm,
    uw_hbm,
    dw_hbm,
    out_ref,
    ow,
    raw,
    turned,
    w,
    qrot,
    inner,
    cumx,
    contrib,
    c_out,
    t_out,
    c_in,
    t_in,
    p_out,
    tt_out,
    p_in,
    tt_in,
    s_own,
    s_out,
    s_in,
    retained,
    mix_out,
    mix_in,
    acc,
    norm_own,
    normed,
    gated,
    hidden,
    keep,
    s1,
    r1,
    s2,
    r2,
    s3,
    r3,
    ow_sem,
    raw_sem,
    own_sem,
    w_send,
    w_recv,
    f_send,
    f_recv,
    cx_send,
    cx_recv,
    pz_send,
    pz_recv,
    sx_send,
    sx_recv,
    mix_send,
    mix_recv,
    nz_send,
    nz_recv,
    nt_send,
    nt_recv,
    t1_send,
    t1_recv,
    t2_send,
    t2_recv,
    t3_send,
    t3_recv,
):
    sp = lax.axis_index("sp")
    tp = lax.axis_index("tp")
    z, x = sp // XS, lax.rem(sp, XS)
    y, c = tp // CS, lax.rem(tp, CS)
    rows = q_ref.shape[0]
    heads = ld_ref.shape[0]
    hh = heads // XS
    hd = q_ref.shape[1] // heads
    quarter = rows // nt
    share, width = w.shape[2], w.shape[3]
    group = XS * width
    x_peer = (z * XS + (1 - x), tp)
    c_peer = (sp, y * CS + (1 - c))
    y_peer = (sp, (1 - y) * CS + c)

    def z_at(d):
        return lax.rem(z + d, nz)

    def z_from(d):
        return lax.rem(z - d + nz, nz)

    def z_peer(d):
        return (z_at(d) * XS + x, tp)

    def t_at(d):
        return lax.rem(tp + d, nt)

    def t_peer(d):
        return (sp, t_at(d))

    def remote(src, dst, send, recv, peer):
        return pltpu.make_async_remote_copy(
            src_ref=src,
            dst_ref=dst,
            send_sem=send,
            recv_sem=recv,
            device_id=peer,
            device_id_type=MESH,
        )

    started = []

    def go(copy):
        copy.start()
        started.append(copy)
        return copy

    def piece(m, zz):
        at = pl.ds(pl.multiple_of(zz * share, 16), share)
        return dw_hbm.at[at] if m == 2 else turned.at[m, at]

    raw_copies = []
    for m, source in enumerate((gw_hbm, uw_hbm)):
        raw_copy = pltpu.make_async_copy(source, raw.at[m], raw_sem.at[m])
        raw_copy.start()
        raw_copies.append(raw_copy)
    ow_copy = pltpu.make_async_copy(ow_hbm, ow, ow_sem)
    own_copies = {}

    def take_own(m):
        own_copies[m] = pltpu.make_async_copy(piece(m, z), w.at[m, sp], own_sem.at[m])
        own_copies[m].start()

    take_own(2)
    ow_copy.start()

    barrier = pltpu.get_barrier_semaphore()
    peers = [z_peer(d) for d in range(1, nz)] + [x_peer] + [t_peer(d) for d in range(1, nt)]
    for peer in peers:
        pl.semaphore_signal(barrier, inc=1, device_id=peer, device_id_type=MESH)
    for m in range(2):
        raw_copies[m].wait()
        for j in range(raw.shape[2] // 128):
            turned[m, j * 128 : (j + 1) * 128, :] = jnp.transpose(
                raw[m, :, j * 128 : (j + 1) * 128]
            )
        take_own(m)
    pl.semaphore_wait(barrier, len(peers))

    w_copies = {}

    def send_weight(m, d):
        w_copies[m, d] = go(
            remote(piece(m, z_at(d)), w.at[m, sp], w_send.at[m, d], w_recv.at[m, d], z_peer(d))
        )

    f_copies = {}

    def forward(m, d):
        slot = z_from(d) * XS + x
        if d == 0:
            own_copies[m].wait()
        else:
            w_copies[m, d].wait_recv()
        f_copies[m, d] = go(
            remote(w.at[m, slot], w.at[m, slot], f_send.at[m, d], f_recv.at[m, d], x_peer)
        )

    far = 2
    near = [d for d in range(1, nz) if d != far]
    send_weight(1, far)

    ti = lax.broadcasted_iota(jnp.int32, (rows, rows), 0)
    si = lax.broadcasted_iota(jnp.int32, (rows, rows), 1)
    lower = si <= ti
    cumul = lax.dot_general(
        ld_ref[...],
        (ti <= si).astype(F32),
        (((1,), (0,)), ((), ())),
        precision=lax.Precision.HIGHEST,
        preferred_element_type=F32,
    )
    half = hd // 2
    lane = lax.broadcasted_iota(jnp.int32, (1, hd), 1)
    low_half = lane < half
    index = jnp.where(low_half, lane, lane - half).astype(F32)
    freq = jnp.exp(index * (-math.log(10000.0) / (half - 1)))
    angles = (sp * rows + lax.broadcasted_iota(jnp.int32, (rows, hd), 0)).astype(F32) * freq
    cos = jnp.cos(angles)
    sin = jnp.sin(angles)
    sin = jnp.where(low_half, -sin, sin)
    for h in range(heads):
        cols = slice(h * hd, (h + 1) * hd)
        qf = q_ref[:, cols].astype(F32)
        kf = k_ref[:, cols].astype(F32)
        vb = v_ref[:, cols]
        qb = (qf * cos + pltpu.roll(qf, half, 1) * sin).astype(BF16)
        kb = ((kf * cos + pltpu.roll(kf, half, 1) * sin) * hd ** (-0.5)).astype(BF16)
        along = jnp.broadcast_to(cumul[h : h + 1, :], (rows, rows))
        cum = jnp.transpose(along)
        spread = cum - along
        weight = jnp.where(lower, jnp.exp(jnp.where(lower, spread, 0.0)), 0.0)
        probs = (dot_nt(qb, kb) * weight).astype(BF16)
        inner[:, cols] = dot_nn(probs, vb)
        last = cum[rows - 1 :, :]
        kw = kb.astype(F32) * jnp.exp(last - cum)
        cb = dot_nn(jnp.transpose(kw).astype(BF16), vb)
        contrib[h] = cb
        c_out[h] = cb.astype(BF16)
        t_out[h] = jnp.broadcast_to(jnp.exp(last), t_out.shape[1:])
        qrot[:, cols] = qb.astype(F32)
        cumx[:, cols] = jnp.exp(cum)
    mine_h, other_h = x * hh, (1 - x) * hh
    cx = go(remote(c_out.at[pl.ds(other_h, hh)], c_in, cx_send.at[0], cx_recv.at[0], x_peer))
    tx = go(remote(t_out, t_in, cx_send.at[1], cx_recv.at[1], x_peer))
    forward(1, 0)
    cx.wait_recv()
    tx.wait_recv()
    first = x == 0
    for i in range(hh):
        own_c, own_t = contrib[mine_h + i], t_out[mine_h + i][:1]
        other_c, other_t = c_in[i].astype(F32), t_in[mine_h + i][:1]
        plane = jnp.where(first, other_t * own_c + other_c, own_t * other_c + own_c)
        p_out[i] = plane.astype(BF16)
        tt_out[i] = jnp.broadcast_to(own_t * other_t, tt_out.shape[1:])
    pz, tz = {}, {}
    for d in range(1, nz):
        pz[d] = go(remote(p_out, p_in.at[z], pz_send.at[0, d], pz_recv.at[0, d], z_peer(d)))
        tz[d] = go(remote(tt_out, tt_in.at[z], pz_send.at[1, d], pz_recv.at[1, d], z_peer(d)))
    for d in range(1, nz):
        pz[d].wait_recv()
        tz[d].wait_recv()
    send_weight(0, far)
    send_weight(0, near[0])
    p_in[z] = p_out[...]
    tt_in[z] = tt_out[...]
    for i in range(hh):
        state = jnp.zeros((hd, hd), F32)
        for zz in range(nz - 1):
            later = tt_in[zz, i][:1] * state + p_in[zz, i].astype(F32)
            state = jnp.where(zz < z, later, state)
        early_t = jnp.where(first, t_out[mine_h + i][:1], t_in[mine_h + i][:1])
        early_c = jnp.where(first, contrib[mine_h + i], c_in[i].astype(F32))
        after = early_t * state + early_c
        s_own[i] = jnp.where(first, state, after)
        s_out[i] = jnp.where(first, after, state).astype(BF16)
    sx = go(remote(s_out, s_in, sx_send, sx_recv, x_peer))
    forward(0, 0)
    forward(1, far)

    def finish(h, state, cols):
        cross = lax.dot_general(
            qrot[:, cols],
            state,
            (((1,), (0,)), ((), ())),
            precision=lax.Precision.HIGHEST,
            preferred_element_type=F32,
        )
        ret = inner[:, cols] + cumx[:, cols] * cross
        scale = lax.rsqrt(jnp.mean(ret * ret, axis=-1, keepdims=True) + EPS)
        gf = g_ref[:, cols].astype(F32)
        retained[:, cols] = (
            ret * scale * hg_ref[:, cols] * (gf / (1.0 + jnp.exp(-gf)))
        ).astype(BF16)

    sx.wait_recv()
    for h in range(heads):
        cols = slice(h * hd, (h + 1) * hd)
        i = h % hh
        mine = x == h // hh
        finish(h, jnp.where(mine, s_own[i], s_in[i].astype(F32)), cols)
    ow_copy.wait()
    mixes = []
    for d in list(range(1, nt)) + [0]:
        mine = pl.multiple_of(t_at(d) * quarter, quarter)
        part = dot_nn(retained[pl.ds(mine, quarter), :], ow[...]).astype(BF16)
        if d == 0:
            mix_in[tp] = part
        else:
            mix_out[d] = part
            mixes.append(
                go(
                    remote(
                        mix_out.at[d], mix_in.at[tp], mix_send.at[d], mix_recv.at[d], t_peer(d)
                    )
                )
            )
    for mix in mixes:
        mix.wait_recv()
    mixed = mix_in[0].astype(F32)
    for j in range(1, nt):
        mixed += mix_in[j].astype(F32)
    mine = pl.multiple_of(tp * quarter, quarter)
    mid = (res_ref[pl.ds(mine, quarter), :].astype(F32) + mixed).astype(BF16).astype(F32)
    for g in range(nz):
        for u in range(XS):
            at = g * group + u * width
            acc[g, u] = mid[:, at : at + width]
    norm_own[...] = (
        mid * lax.rsqrt(jnp.mean(mid * mid, axis=-1, keepdims=True) + EPS) * mg_ref[...]
    ).astype(BF16)
    normed[z, tp] = norm_own[...]
    tcopy = {}

    def share_rows(i, zz):
        rows_at = normed.at[zz, tp]
        for e, peer in ((1, c_peer), (2, y_peer)):
            tcopy[i, e] = go(
                remote(rows_at, rows_at, nt_send.at[i, e], nt_recv.at[i, e], peer)
            )

    def pass_rows(i, zz):
        rows_at = normed.at[zz, (1 - y) * CS + c]
        tcopy[i, 2].wait_recv()
        tcopy[i, 3] = go(remote(rows_at, rows_at, nt_send.at[i, 3], nt_recv.at[i, 3], c_peer))

    mate = z + 1 - 2 * lax.rem(z, 2)
    mate_peer = (mate * XS + x, tp)
    z_far, z_last = z_from(far), lax.rem(mate + far, nz)
    n_far = go(remote(norm_own, normed.at[z, tp], nz_send.at[0], nz_recv.at[0], z_peer(far)))
    n_mate = go(remote(norm_own, normed.at[z, tp], nz_send.at[1], nz_recv.at[1], mate_peer))
    share_rows(0, z)
    forward(0, far)
    forward(2, 0)
    n_far.wait_recv()
    far_rows = normed.at[z_far, tp]
    n_pass = go(remote(far_rows, far_rows, nz_send.at[2], nz_recv.at[2], mate_peer))
    share_rows(1, z_far)
    send_weight(0, near[1])
    for d in near:
        send_weight(1, d)
    for d in [far] + near:
        send_weight(2, d)
    forward(0, near[0])
    n_mate.wait_recv()
    share_rows(2, mate)
    pass_rows(0, z)
    pass_rows(1, z_far)
    n_pass.wait_recv()
    share_rows(3, z_last)
    pass_rows(2, mate)
    forward(0, near[1])
    pass_rows(3, z_last)
    forward(1, near[0])
    for d in range(nz):
        f_copies[0, d].wait_recv()
    for key in sorted(tcopy):
        if key[1] != 2:
            tcopy[key].wait_recv()

    ns = nz * XS

    def project(m, zz):
        block = normed[zz].reshape(rows, normed.shape[3])
        total = dot_nt(block[:, :width], w[m, 0])
        for s in range(1, ns):
            total += dot_nt(block[:, s * width : (s + 1) * width], w[m, s])
        return total

    def gate_rows(zz):
        gate = project(0, zz)
        gated[zz] = gate / (1.0 + jnp.exp(-gate))

    def up_rows(zz):
        hidden[zz * rows : (zz + 1) * rows, :] = (gated[zz] * project(1, zz)).astype(BF16)

    for zz in range(nz // 2):
        gate_rows(zz)
    forward(1, near[1])
    for zz in range(nz // 2, nz):
        gate_rows(zz)
    forward(2, far)
    for d in range(nz):
        f_copies[1, d].wait_recv()
    for zz in range(nz):
        up_rows(zz)

    t1, t2, t3 = {}, {}, {}
    low = c == 0

    def side(u):
        return x if u == 0 else 1 - x

    def compute(b, u):
        if u:
            f_copies[2, b].wait_recv()
        part = dot_nn(hidden[...], w[2, z_from(b) * XS + side(u)])
        for zz in range(nz):
            for yy in range(nt // CS):
                at = zz * rows + yy * CS * quarter
                even = part[at : at + quarter]
                odd = part[at + quarter : at + 2 * quarter]
                keep[b, u, yy, zz] = jnp.where(low, even, odd)
                s1[b, u, yy, zz] = jnp.where(low, odd, even).astype(BF16)
        t1[b, u] = go(
            remote(s1.at[b, u], r1.at[b, u], t1_send.at[b, u], t1_recv.at[b, u], c_peer)
        )

    def second(b, u):
        t1[b, u].wait_recv()
        s2[b, u] = (keep[b, u, 1 - y] + r1[b, u, 1 - y].astype(F32)).astype(BF16)
        t2[b, u] = go(
            remote(s2.at[b, u], r2.at[b, u], t2_send.at[b, u], t2_recv.at[b, u], y_peer)
        )
        keep[b, u, y] = keep[b, u, y] + r1[b, u, y].astype(F32)

    def third(b, u):
        t2[b, u].wait_recv()
        for e in [far] + near:
            zz = z_at(e)
            s3[b, u, e] = (keep[b, u, y, zz] + r2[b, u, zz].astype(F32)).astype(BF16)
            t3[b, u, e] = go(
                remote(
                    s3.at[b, u, e],
                    r3.at[b, u, e],
                    t3_send.at[b, u, e],
                    t3_recv.at[b, u, e],
                    z_peer(e),
                )
            )
        g, v = z_from(b), side(u)
        acc[g, v] = acc[g, v] + keep[b, u, y, z] + r2[b, u, z].astype(F32)

    n0, n1 = near
    compute(0, 0)
    compute(0, 1)
    compute(far, 0)
    second(0, 0)
    second(0, 1)
    forward(2, n0)
    compute(n0, 0)
    compute(far, 1)
    second(far, 0)
    forward(2, n1)
    compute(n1, 0)
    second(n0, 0)
    second(far, 1)
    third(0, 0)
    third(0, 1)
    second(n1, 0)
    compute(n0, 1)
    third(far, 0)
    third(n0, 0)
    second(n0, 1)
    compute(n1, 1)
    third(far, 1)
    second(n1, 1)
    third(n1, 0)
    third(n0, 1)
    third(n1, 1)
    order = [(0, 0), (0, 1), (far, 0), (n0, 0), (far, 1), (n1, 0), (n0, 1), (n1, 1)]
    for b, u in order:
        for e in [far] + near:
            t3[b, u, e].wait_recv()
            g, v = lax.rem(z - e - b + 2 * nz, nz), side(u)
            acc[g, v] = acc[g, v] + r3[b, u, e].astype(F32)
    for g in range(nz):
        for u in range(XS):
            at = g * group + u * width
            out_ref[:, at : at + width] = acc[g, u].astype(BF16)
    for copy in started:
        copy.wait_send()


def fast_body(
    queries,
    key_rows,
    value_rows,
    gate_input,
    log_decay,
    head_gain,
    out_weight,
    residual,
    mlp_gain,
    gate_weight,
    up_weight,
    down_weight,
):
    rows, wide = queries.shape
    heads = log_decay.shape[1]
    hd = wide // heads
    model = residual.shape[1]
    ns, nt = lax.axis_size("sp"), lax.axis_size("tp")
    nz = ns // XS
    quarter = rows // nt
    width, units = gate_weight.shape
    share = units // nz
    group = XS * width
    hh = heads // XS
    vmem = pl.BlockSpec(memory_space=pltpu.VMEM)
    anyspace = pl.BlockSpec(memory_space=pl.ANY)
    dma = pltpu.SemaphoreType.DMA
    scratch = [
        pltpu.VMEM(out_weight.shape, BF16),
        pltpu.VMEM((2, width, units), BF16),
        pltpu.VMEM((2, units, width), BF16),
        pltpu.VMEM((3, ns, share, width), BF16),
        pltpu.VMEM((rows, wide), F32),
        pltpu.VMEM((rows, wide), F32),
        pltpu.VMEM((rows, wide), F32),
        pltpu.VMEM((heads, hd, hd), F32),
        pltpu.VMEM((heads, hd, hd), BF16),
        pltpu.VMEM((heads, 8, hd), F32),
        pltpu.VMEM((hh, hd, hd), BF16),
        pltpu.VMEM((heads, 8, hd), F32),
        pltpu.VMEM((hh, hd, hd), BF16),
        pltpu.VMEM((hh, 8, hd), F32),
        pltpu.VMEM((nz, hh, hd, hd), BF16),
        pltpu.VMEM((nz, hh, 8, hd), F32),
        pltpu.VMEM((hh, hd, hd), F32),
        pltpu.VMEM((hh, hd, hd), BF16),
        pltpu.VMEM((hh, hd, hd), BF16),
        pltpu.VMEM((rows, wide), BF16),
        pltpu.VMEM((nt, quarter, model), BF16),
        pltpu.VMEM((nt, quarter, model), BF16),
        pltpu.VMEM((nz, XS, quarter, width), F32),
        pltpu.VMEM((quarter, model), BF16),
        pltpu.VMEM((nz, nt, quarter, model), BF16),
        pltpu.VMEM((nz, rows, share), F32),
        pltpu.VMEM((nz * rows, share), BF16),
        pltpu.VMEM((nz, XS, nt // CS, nz, quarter, width), F32),
        pltpu.VMEM((nz, XS, nt // CS, nz, quarter, width), BF16),
        pltpu.VMEM((nz, XS, nt // CS, nz, quarter, width), BF16),
        pltpu.VMEM((nz, XS, nz, quarter, width), BF16),
        pltpu.VMEM((nz, XS, nz, quarter, width), BF16),
        pltpu.VMEM((nz, XS, nz, quarter, width), BF16),
        pltpu.VMEM((nz, XS, nz, quarter, width), BF16),
        dma,
        dma((2,)),
        dma((3,)),
        dma((3, nz)),
        dma((3, nz)),
        dma((3, nz)),
        dma((3, nz)),
        dma((2,)),
        dma((2,)),
        dma((2, nz)),
        dma((2, nz)),
        dma,
        dma,
        dma((nt,)),
        dma((nt,)),
        dma((nz,)),
        dma((nz,)),
        dma((nz, nt)),
        dma((nz, nt)),
        dma((nz, XS)),
        dma((nz, XS)),
        dma((nz, XS)),
        dma((nz, XS)),
        dma((nz, XS, nz)),
        dma((nz, XS, nz)),
    ]
    return pl.pallas_call(
        functools.partial(kernel, nz, nt),
        out_shape=jax.ShapeDtypeStruct((quarter, model), BF16),
        in_specs=[vmem] * 8 + [anyspace] * 4,
        out_specs=vmem,
        scratch_shapes=scratch,
        compiler_params=pltpu.CompilerParams(
            collective_id=0, has_side_effects=True, vmem_limit_bytes=60 * 1024 * 1024
        ),
    )(
        queries,
        key_rows,
        value_rows,
        gate_input,
        log_decay.T,
        head_gain.reshape(1, wide),
        residual,
        mlp_gain.reshape(1, model),
        out_weight,
        gate_weight,
        up_weight,
        down_weight,
    )


def fits(mesh, queries, log_decay, gate_weight):
    ns, nt = mesh.shape["sp"], mesh.shape["tp"]
    tokens, wide = queries.shape
    if ns % XS or ns // XS != 4 or nt != 2 * CS or tokens // ns != BLOCK:
        return False
    nz = ns // XS
    hidden = gate_weight.shape[1] // nt
    return (
        gate_weight.shape[0] // ns % 128 == 0
        and hidden % (16 * nz) == 0
        and wide // log_decay.shape[1] == 128
        and BLOCK % (16 * nt) == 0
        and hidden % 128 == 0
        and log_decay.shape[1] // nt % XS == 0
    )


def solution(mesh):
    def run(*args):
        good = fits(mesh, args[0], args[4], args[9])
        return jax.shard_map(
            fast_body if good else body,
            mesh=mesh,
            in_specs=(
                P("sp", "tp"),
                P("sp", "tp"),
                P("sp", "tp"),
                P("sp", "tp"),
                P("sp", "tp"),
                P("tp"),
                P("tp", None),
                P("sp", None),
                P(),
                P("sp", "tp"),
                P("sp", "tp"),
                P("tp", "sp"),
            ),
            out_specs=P(("sp", "tp"), None),
            check_vma=False,
        )(*args)

    return run
```

profile of v0, /device:TPU:0, one launch (start us, length us, event | category | flops | bytes accessed | tf_op | source)
XLA Modules:
  0.0 95.6 jit_solution(5405048690658384560)
XLA Ops:
  0.0 94.0 %shard_map.118 = bf16[32,2048]{1,0:T(8,128)(2,1)} custom-call(bf16[128,512]{1,0:T(8,128)(2,1)} %q_ref.1, bf16[128,512]{1,0:T(8,128)(2,1)} %k_ref.1, bf16[128,512]{1,0:T(8,128)(2,1)} %v_ref.1, bf16[128,512]{1,0:T(8,128)(2,1)} %g_ref.1, f32[4,128]{1,0:T(4,128)} %bitcast.4, f32[1,512]{1,0:T(1,128)} %bitcast.5, bf16[128,2048]{1,0:T(8,128)(2,1)} %res_ref.1, ...), custom_call_target="tpu_custom_call" | custom-call | tf_op jit(solution)/shard_map/pallas_call | solution.py:731
  94.1 1.6 %copy.14 = bf16[32,2048]{1,0:T(8,128)(2,1)} copy(bf16[32,2048]{1,0:T(8,128)(2,1)} %shard_map.118) | data formatting | bytes 262144
where the time goes:
time: 95.8 us; the launch traced here: 95.6 us
  Pallas kernels  94 us (98%)
  local copies, waits for them, and re-layouts  1.57 us (2%)
    pallas_call x1, Pallas kernels, fast_body(): pl.pallas_call(functools.partial(kernel, nz, nt), out_shape=jax.ShapeDtyp...  94 us

commit v1 on v0

v1 whole, which is shorter than its diff:
```python
import functools
import math
import types

import jax
import jax.numpy as jnp
from jax import lax
from jax.experimental import pallas as pl
from jax.experimental.pallas import tpu as pltpu
from jax.sharding import PartitionSpec as P

BLOCK = 128


EPS = 1e-06


def prefix_2(x, axis, join, neutral):
    place = lax.axis_index(axis)
    gathered = jax.tree.map(
        lambda a, kind: lax.all_gather(a.astype(kind), axis), x, (jnp.bfloat16, jnp.bfloat16)
    )
    state = jax.tree.map(lambda a, e: jnp.zeros_like(a) + jnp.asarray(e, a.dtype), x, neutral)

    def one(step, state):
        return join(
            state,
            jax.tree.map(
                lambda a, own: lax.dynamic_index_in_dim(a, step, 0, False).astype(own.dtype),
                gathered,
                x,
            ),
        )

    return lax.fori_loop(0, place, one, state)


def rotate(values_in, positions):
    half = values_in.shape[-1] // 2
    freq = 10000.0 ** (-jnp.linspace(0.0, 1.0, half, dtype=jnp.float32))
    angles = positions * freq
    angles = jnp.concatenate([angles, angles], axis=-1)
    first = values_in[..., :half]
    second = values_in[..., half:]
    turned = jnp.concatenate([-second, first], axis=-1)
    return values_in * jnp.cos(angles) + turned * jnp.sin(angles)


def row_norm(stream, gain):
    return stream * lax.rsqrt(jnp.mean(stream * stream, axis=-1, keepdims=True) + EPS) * gain


def join_states(earlier, later):
    return (earlier[0] * later[0], later[0][:, None, None] * earlier[1] + later[1])


def body(
    queries,
    key_rows,
    value_rows,
    gate_input,
    log_decay,
    head_gain,
    out_weight,
    residual,
    mlp_gain,
    gate_weight,
    up_weight,
    down_weight,
):
    tok_rows = queries.shape[0]
    heads_here = log_decay.shape[1]
    head_size = head_gain.shape[0] // heads_here
    quarter = tok_rows // lax.axis_size("tp")
    offset = lax.axis_index("sp") * tok_rows
    positions = (offset + lax.iota(jnp.int32, tok_rows)).astype(jnp.float32)[:, None, None]
    q_rot = rotate(
        queries.reshape(tok_rows, heads_here, head_size).astype(jnp.float32), positions
    ).astype(jnp.bfloat16)
    k_rot = (
        rotate(key_rows.reshape(tok_rows, heads_here, head_size).astype(jnp.float32), positions)
        * head_size ** (-0.5)
    ).astype(jnp.bfloat16)
    blocks = tok_rows // BLOCK
    q_blocks = q_rot.reshape(blocks, BLOCK, heads_here, head_size)
    k_blocks = k_rot.reshape(blocks, BLOCK, heads_here, head_size)
    v_blocks = value_rows.reshape(blocks, BLOCK, heads_here, head_size)
    cumul = jnp.cumsum(log_decay.reshape(blocks, BLOCK, heads_here), axis=1)
    by_head = cumul.transpose(0, 2, 1)
    lower = jnp.tril(jnp.ones((BLOCK, BLOCK), dtype=bool))
    spread = by_head[:, :, :, None] - by_head[:, :, None, :]
    weight = jnp.where(lower, jnp.exp(jnp.where(lower, spread, 0.0)), 0.0)
    scores = jnp.einsum("nthd,nshd->nhts", q_blocks, k_blocks, preferred_element_type=jnp.float32)
    probs = (scores * weight).astype(jnp.bfloat16)
    inner = jnp.einsum("nhts,nshe->nthe", probs, v_blocks, preferred_element_type=jnp.float32)
    k_weighted = (
        k_blocks.astype(jnp.float32) * jnp.exp(cumul[:, -1:, :] - cumul)[..., None]
    ).astype(jnp.bfloat16)
    contrib = jnp.einsum(
        "nshd,nshe->nhde", k_weighted, v_blocks, preferred_element_type=jnp.float32
    )
    totals = jnp.exp(cumul[:, -1, :])

    def advance(carry, items):
        state, prefix = carry
        factor, update = items
        return ((state * factor[:, None, None] + update, prefix * factor), (state, prefix))

    start_state = jnp.zeros((heads_here, head_size, head_size), jnp.float32)
    start_prefix = jnp.ones((heads_here,), jnp.float32)
    (dev_state, dev_total), (local_before, prefixes) = lax.scan(
        advance, (start_state, start_prefix), (totals, contrib)
    )
    _, incoming = prefix_2((dev_total, dev_state), "sp", join_states, (start_prefix, start_state))
    before = local_before + prefixes[:, :, None, None] * incoming[None]
    cross = jnp.einsum(
        "nthd,nhde->nthe", q_blocks.astype(jnp.float32), before, precision=lax.Precision.HIGHEST
    )
    cross = cross * jnp.exp(cumul)[..., None]
    result = (inner + cross).reshape(tok_rows, heads_here, head_size)
    result = row_norm(result, head_gain.reshape(heads_here, head_size)).reshape(
        tok_rows, heads_here * head_size
    )
    retained = (result * jax.nn.silu(gate_input.astype(jnp.float32))).astype(jnp.bfloat16)
    picked = retained
    mixed = lax.psum_scatter(
        jnp.dot(picked, out_weight, preferred_element_type=jnp.float32).astype(jnp.bfloat16),
        "tp",
        scatter_dimension=0,
        tiled=True,
    ).astype(jnp.float32)
    own_rows = lax.dynamic_slice_in_dim(residual, lax.axis_index("tp") * quarter, quarter, 0)
    rows_mid = (own_rows.astype(jnp.float32) + mixed).astype(jnp.bfloat16)
    own_normed = row_norm(rows_mid.astype(jnp.float32), mlp_gain).astype(jnp.bfloat16)
    normed = lax.all_gather(own_normed, "tp", axis=0, tiled=True)
    gate = jnp.dot(
        normed,
        lax.all_gather(gate_weight, "sp", axis=0, tiled=True),
        preferred_element_type=jnp.float32,
    )
    upvals = jnp.dot(
        normed,
        lax.all_gather(up_weight, "sp", axis=0, tiled=True),
        preferred_element_type=jnp.float32,
    )
    full_down = lax.all_gather(down_weight, "sp", axis=1, tiled=True)
    hidden = (jax.nn.silu(gate) * upvals).astype(jnp.bfloat16)
    picked = hidden
    ffn = lax.psum_scatter(
        jnp.dot(picked, full_down, preferred_element_type=jnp.float32).astype(jnp.bfloat16),
        "tp",
        scatter_dimension=0,
        tiled=True,
    ).astype(jnp.float32)
    return (rows_mid.astype(jnp.float32) + ffn).astype(jnp.bfloat16)


MESH = pl.DeviceIdType.MESH
XS = 2
CS = 2
F32 = jnp.float32
BF16 = jnp.bfloat16


def dot_nt(a, b):
    return lax.dot_general(a, b, (((1,), (1,)), ((), ())), preferred_element_type=F32)


def dot_nn(a, b):
    return lax.dot_general(a, b, (((1,), (0,)), ((), ())), preferred_element_type=F32)


def kernel(names, nz, nt, *refs):
    r = types.SimpleNamespace(**dict(zip(names, refs)))
    sp = lax.axis_index("sp")
    tp = lax.axis_index("tp")
    z, x = sp // XS, lax.rem(sp, XS)
    y, c = tp // CS, lax.rem(tp, CS)
    rows = r.q.shape[0]
    heads = r.ld.shape[0]
    hh = heads // XS
    hd = r.q.shape[1] // heads
    quarter = rows // nt
    share, width = r.wg.shape[2], r.wg.shape[3]
    group = XS * width
    ns = nz * XS
    zat = [z, z + 1 - 2 * lax.rem(z, 2), lax.rem(z + 2, nz), nz - 1 - z]

    def dev(zz, xx, yy, cc):
        return (zz * XS + xx, yy * CS + cc)

    x_peer = dev(z, 1 - x, y, c)
    c_peer = dev(z, x, y, 1 - c)

    barrier = pltpu.get_barrier_semaphore()
    peers = [dev(zat[e], x, y, k) for e in range(1, nz) for k in range(CS)]
    peers += [c_peer, dev(zat[2], 1 - x, y, c), dev(zat[1], x, 1 - y, c)]
    peers += [dev(z, 1 - x, y, k) for k in range(CS)]
    peers += [dev(z, x, 1 - y, k) for k in range(CS)]
    for peer in peers:
        pl.semaphore_signal(barrier, inc=1, device_id=peer, device_id_type=MESH)

    loads = {}

    def load(name, src, dst):
        loads[name] = pltpu.make_async_copy(src, dst, r.in_sem.at[len(loads)])
        loads[name].start()

    load("gw", r.gw_hbm, r.raw.at[0])
    load("uw", r.uw_hbm, r.raw.at[1])
    for name in ("ld", "q", "k", "v"):
        load(name, getattr(r, name + "_hbm"), getattr(r, name))
    load("dw", r.dw_hbm, r.slab.at[2])
    for name in ("g", "hg", "ow", "mg"):
        load(name, getattr(r, name + "_hbm"), getattr(r, name))
    mine = pl.multiple_of(tp * quarter, quarter)
    load("res", r.res_hbm.at[pl.ds(mine, quarter)], r.res)

    def remote(src, dst, send, recv, peer):
        return pltpu.make_async_remote_copy(
            src_ref=src,
            dst_ref=dst,
            send_sem=send,
            recv_sem=recv,
            device_id=peer,
            device_id_type=MESH,
        )

    started = {}

    def go(build, guard=None):
        build().start()
        started.setdefault(guard, []).append(build)
        return build

    guards = {"c0": c == 0, "c1": c == 1, "up": jnp.logical_and(c == 1, z < nz - 1)}

    def piece(ref, m, zz):
        return ref.at[m, pl.ds(pl.multiple_of(zz * share, 16), share)]

    def slot(m, zz):
        return r.w2.at[zz] if m == 2 else r.wg.at[m, zz * XS + x]

    own_copies = {}

    def take_own(m):
        own_copies[m] = pltpu.make_async_copy(piece(r.slab, m, z), slot(m, z), r.own_sem.at[m])
        own_copies[m].start()

    for m, name in enumerate(("gw", "uw")):
        loads[name].wait()
        for j in range(r.raw.shape[2] // 128):
            r.slab[m, j * 128 : (j + 1) * 128, :] = jnp.transpose(
                r.raw[m, :, j * 128 : (j + 1) * 128]
            )
        take_own(m)
    loads["dw"].wait()
    take_own(2)
    pl.semaphore_wait(barrier, len(peers))

    def hand(m):
        return lambda: remote(
            r.slab.at[m], r.partner.at[m], r.h_send.at[m], r.h_recv.at[m], c_peer
        )

    def weight(m, e, k):
        source = r.partner if k else r.slab
        return lambda: remote(
            piece(source, m, zat[e]),
            slot(m, z),
            r.w_send.at[k, m, e],
            r.w_recv.at[m, e],
            dev(zat[e], x, y, k),
        )

    started["c0"] = [
        weight(m, e, k) for m in range(3) for e in range(1, nz) for k in range(CS)
    ]
    outer = jnp.logical_or(z == 0, z == nz - 1)
    outer_plan = ((0, 1), (1, 1), (0, 2), (0, 3), (2, 1), (1, 2), (1, 3))
    inner_head = ((0, 3), (0, 1), (1, 3), (1, 1))
    inner_tail = ((0, 2), (2, 1), (1, 2))

    def send_weights(plan, which=range(CS)):
        for m, e in plan:
            for k in which:
                weight(m, e, k)().start()

    def got_weight(m, e):
        weight(m, e, 0)().wait_recv()

    def forward(m, e):
        at = slot(m, zat[e])
        source = piece(r.slab, m, z) if e == 0 else at
        return lambda: remote(source, at, r.f_send.at[m, e], r.f_recv.at[m, e], x_peer)

    def pass_on(m, e):
        if e:
            got_weight(m, e)
        go(forward(m, e))

    @pl.when(c == 1)
    def _():
        for m in range(3):
            go(hand(m), "c1")

    @pl.when(jnp.logical_and(c == 0, jnp.logical_not(outer)))
    def _():
        send_weights(inner_head, (0,))

    for name in ("ld", "q", "k", "v"):
        loads[name].wait()
    ti = lax.broadcasted_iota(jnp.int32, (rows, rows), 0)
    si = lax.broadcasted_iota(jnp.int32, (rows, rows), 1)
    lower = si <= ti
    cumul = lax.dot_general(
        r.ld[...],
        (ti <= si).astype(F32),
        (((1,), (0,)), ((), ())),
        precision=lax.Precision.HIGHEST,
        preferred_element_type=F32,
    )
    half = hd // 2
    lane = lax.broadcasted_iota(jnp.int32, (1, hd), 1)
    low_half = lane < half
    index = jnp.where(low_half, lane, lane - half).astype(F32)
    freq = jnp.exp(index * (-math.log(10000.0) / (half - 1)))
    angles = (sp * rows + lax.broadcasted_iota(jnp.int32, (rows, hd), 0)).astype(F32) * freq
    cos = jnp.cos(angles)
    sin = jnp.sin(angles)
    sin = jnp.where(low_half, -sin, sin)
    for h in range(heads):
        cols = slice(h * hd, (h + 1) * hd)
        qf = r.q[:, cols].astype(F32)
        kf = r.k[:, cols].astype(F32)
        vb = r.v[:, cols]
        qb = (qf * cos + pltpu.roll(qf, half, 1) * sin).astype(BF16)
        kb = ((kf * cos + pltpu.roll(kf, half, 1) * sin) * hd ** (-0.5)).astype(BF16)
        along = jnp.broadcast_to(cumul[h : h + 1, :], (rows, rows))
        cum = jnp.transpose(along)
        spread = cum - along
        weight_ts = jnp.where(lower, jnp.exp(jnp.where(lower, spread, 0.0)), 0.0)
        probs = (dot_nt(qb, kb) * weight_ts).astype(BF16)
        r.inner[:, cols] = dot_nn(probs, vb)
        last = cum[rows - 1 :, :]
        kw = kb.astype(F32) * jnp.exp(last - cum)
        r.c_out[h] = dot_nn(jnp.transpose(kw).astype(BF16), vb).astype(BF16)
        r.t_out[h] = jnp.broadcast_to(jnp.exp(last), r.t_out.shape[1:])
        r.qrot[:, cols] = qb
        r.cumx[:, cols] = jnp.exp(cum)

    my_h, its_h = pl.ds(x * hh, hh), pl.ds((1 - x) * hh, hh)
    x_one, c_one = dev(z, 1 - x, y, 1), dev(z, x, y, 1)

    def cross_c(k):
        return lambda: remote(
            r.c_out.at[its_h], r.ci.at[1, k], r.cx_send.at[0], r.cx_recv.at[0, k], x_one
        )

    def cross_t(k):
        return lambda: remote(
            r.t_out.at[its_h], r.ti.at[1, k], r.cx_send.at[1], r.cx_recv.at[1, k], x_one
        )

    go(cross_c(c))
    go(cross_t(c))

    def near_c():
        return remote(r.c_out.at[my_h], r.ci.at[0, 0], r.cc_send.at[0], r.cc_recv.at[0], c_one)

    def near_t():
        return remote(r.t_out.at[my_h], r.ti.at[0, 0], r.cc_send.at[1], r.cc_recv.at[1], c_one)

    def chain():
        up = jnp.minimum(z + 1, nz - 1)
        return remote(r.ch_out, r.ch_in, r.ch_send, r.ch_recv, dev(up, x, y, 1))

    def state_x(k):
        return lambda: remote(
            r.so.at[1, k], r.s_in.at[1], r.so_send.at[k], r.s_recv.at[1], dev(z, 1 - x, y, k)
        )

    def state_c():
        return remote(
            r.so.at[0, 0], r.s_in.at[0], r.so_send.at[2], r.s_recv.at[0], dev(z, x, y, 0)
        )

    @pl.when(c == 0)
    def _():
        go(near_c, "c0")
        go(near_t, "c0")
        for m in range(3):
            hand(m)().wait_recv()

        @pl.when(outer)
        def _():
            send_weights(outer_plan)

        @pl.when(jnp.logical_not(outer))
        def _():
            send_weights(inner_head, (1,))
            send_weights(inner_tail)

    pass_on(0, 0)
    pass_on(1, 0)
    first = x == 0

    @pl.when(c == 1)
    def _():
        r.ci[0, 1] = r.c_out[my_h]
        r.ti[0, 1] = r.t_out[my_h]
        near_c().wait_recv()
        near_t().wait_recv()
        for k in range(CS):
            cross_c(k)().wait_recv()
            cross_t(k)().wait_recv()
        for k in range(CS):
            for i in range(hh):
                own_c, own_t = r.ci[0, k, i].astype(F32), r.ti[0, k, i][:1]
                other_c, other_t = r.ci[1, k, i].astype(F32), r.ti[1, k, i][:1]
                early_c = jnp.where(first, own_c, other_c)
                late_c = jnp.where(first, other_c, own_c)
                late_t = jnp.where(first, other_t, own_t)
                r.plane[k, i] = late_t * early_c + late_c

        @pl.when(z == 0)
        def _():
            r.ch_in[...] = jnp.zeros(r.ch_in.shape, BF16)

        @pl.when(z > 0)
        def _():
            chain().wait_recv()

        for k in range(CS):
            for i in range(hh):
                both_t = r.ti[0, k, i][:1] * r.ti[1, k, i][:1]
                state = r.ch_in[k, i].astype(F32)
                r.ch_out[k, i] = (both_t * state + r.plane[k, i]).astype(BF16)

        @pl.when(z < nz - 1)
        def _():
            go(chain, "up")

        for k in range(CS):
            for i in range(hh):
                early_c = jnp.where(first, r.ci[0, k, i], r.ci[1, k, i]).astype(F32)
                early_t = jnp.where(first, r.ti[0, k, i][:1], r.ti[1, k, i][:1])
                state = r.ch_in[k, i].astype(F32)
                after = early_t * state + early_c
                r.so[0, k, i] = jnp.where(first, state, after).astype(BF16)
                r.so[1, k, i] = jnp.where(first, after, state).astype(BF16)
        for k in range(CS):
            go(state_x(k), "c1")
        go(state_c, "c1")
        r.s_in[0] = r.so[0, 1]

    @pl.when(c == 0)
    def _():
        state_c().wait_recv()

    state_x(0)().wait_recv()
    loads["g"].wait()
    loads["hg"].wait()
    for h in range(heads):
        cols = slice(h * hd, (h + 1) * hd)
        state = r.s_in[lax.rem(x + h // hh, XS), h % hh]
        ret = r.inner[:, cols] + r.cumx[:, cols] * dot_nn(r.qrot[:, cols], state)
        scale = lax.rsqrt(jnp.mean(ret * ret, axis=-1, keepdims=True) + EPS)
        gf = r.g[:, cols].astype(F32)
        r.retained[:, cols] = (
            ret * scale * r.hg[:, cols] * (gf / (1.0 + jnp.exp(-gf)))
        ).astype(BF16)
    loads["ow"].wait()

    def mix_c():
        return remote(r.mc_out, r.mc_in, r.mix_send.at[0], r.mix_recv.at[0], c_peer)

    def mix_y():
        return remote(
            r.my_out, r.my_in, r.mix_send.at[1], r.mix_recv.at[1], dev(z, x, 1 - y, c)
        )

    def mix_part(cc):
        picked = [
            r.retained[pl.ds(pl.multiple_of((yy * CS + cc) * quarter, quarter), quarter), :]
            for yy in range(nt // CS)
        ]
        part = dot_nn(jnp.concatenate(picked, axis=0), r.ow[...])
        return part.reshape(nt // CS, quarter, part.shape[1])

    r.mc_out[...] = mix_part(1 - c).astype(BF16)
    go(mix_c)
    r.mix_own[...] = mix_part(c)
    mix_c().wait_recv()
    r.my_out[...] = (r.mix_own[1 - y] + r.mc_in[1 - y].astype(F32)).astype(BF16)
    go(mix_y)
    pass_on(0, 1)
    mixed = r.mix_own[y] + r.mc_in[y].astype(F32)
    mix_y().wait_recv()
    mixed += r.my_in[...].astype(F32)
    loads["res"].wait()
    loads["mg"].wait()
    mid = (r.res[...].astype(F32) + mixed).astype(BF16).astype(F32)
    for g in range(nz):
        for u in range(XS):
            at = g * group + u * width
            r.acc[g, u] = mid[:, at : at + width]
    r.normed[z, tp] = (
        mid * lax.rsqrt(jnp.mean(mid * mid, axis=-1, keepdims=True) + EPS) * r.mg[...]
    ).astype(BF16)

    def rows_c():
        rows_at = r.normed.at[z, tp]
        return remote(rows_at, rows_at, r.nc_send, r.nc_recv, c_peer)

    def pair(zz, yy):
        return r.normed.at[zz, pl.ds(yy * CS, CS)]

    def rows_z(k):
        to = zat[2] if k == 0 else zat[1]
        zz = zat[2] if k == 2 else z
        return lambda: remote(
            pair(zz, y), pair(zz, y), r.nz_send.at[k], r.nz_recv.at[k], dev(to, x, y, 1)
        )

    def rows_y(e):
        return lambda: remote(
            pair(zat[e], y),
            pair(zat[e], y),
            r.ny_send.at[e],
            r.ny_recv.at[e],
            dev(z, x, 1 - y, 1),
        )

    def rows_d(e, v):
        def build():
            rows_at = pair(zat[e], 1 - y if v else y)
            return remote(
                rows_at, rows_at, r.nd_send.at[v, e], r.nd_recv.at[v, e], dev(z, x, y, 0)
            )

        return build

    go(rows_c)
    rows_c().wait_recv()

    @pl.when(c == 1)
    def _():
        for k in range(2):
            go(rows_z(k), "c1")
        go(rows_y(0), "c1")

    pass_on(1, 1)
    pass_on(0, 2)

    @pl.when(c == 1)
    def _():
        rows_z(1)().wait_recv()
        go(rows_y(1), "c1")
        go(rows_d(1, 0), "c1")
        rows_y(0)().wait_recv()
        go(rows_d(0, 1), "c1")
        rows_z(0)().wait_recv()
        go(rows_z(2), "c1")
        go(rows_y(2), "c1")
        go(rows_d(2, 0), "c1")

    pass_on(0, 3)
    pass_on(1, 3)

    def send_down(if_outer, if_inner):
        @pl.when(outer)
        def _():
            send_weights(((2, if_outer),))

        @pl.when(jnp.logical_not(outer))
        def _():
            send_weights(((2, if_inner),))

    @pl.when(c == 1)
    def _():
        rows_y(1)().wait_recv()
        go(rows_d(1, 1), "c1")
        rows_z(2)().wait_recv()
        go(rows_y(3), "c1")
        go(rows_d(3, 0), "c1")
        rows_y(2)().wait_recv()
        go(rows_d(2, 1), "c1")
        rows_y(3)().wait_recv()
        go(rows_d(3, 1), "c1")

    @pl.when(c == 0)
    def _():
        rows_d(2, 0)().wait_recv()
        send_down(2, 3)

    pass_on(1, 2)

    @pl.when(c == 0)
    def _():
        rows_d(3, 0)().wait_recv()
        send_down(3, 2)
        rows_d(1, 0)().wait_recv()
        for e in range(nz):
            rows_d(e, 1)().wait_recv()

    def project(m, lo, hi):
        block = r.normed[lo:hi].reshape((hi - lo) * rows, r.normed.shape[3])
        total = dot_nt(block[:, :width], r.wg[m, 0])
        for s in range(1, ns):
            total += dot_nt(block[:, s * width : (s + 1) * width], r.wg[m, s])
        return total

    def hand_hidden(i):
        at = pl.ds(i * 2 * rows, 2 * rows)
        return lambda: remote(
            r.hidden.at[0, at], r.hidden.at[1, at], r.hx_send.at[i], r.hx_recv.at[i], x_peer
        )

    own_copies[0].wait()
    for e in range(nz):
        forward(0, e)().wait_recv()
    for i in range(nz // 2):
        gate = project(0, 2 * i, 2 * i + 2)
        r.gated[i] = gate / (1.0 + jnp.exp(-gate))
    own_copies[1].wait()
    for e in range(nz):
        forward(1, e)().wait_recv()
    for i in range(nz // 2):
        at = slice(i * 2 * rows, (i + 1) * 2 * rows)
        r.hidden[0, at, :] = (r.gated[i] * project(1, 2 * i, 2 * i + 2)).astype(BF16)
        go(hand_hidden(i))
    own_copies[2].wait()

    low = c == 0

    def t1(b, u):
        return lambda: remote(
            r.s1.at[b, u], r.r1.at[b, u], r.t1_send.at[b, u], r.t1_recv.at[b, u], c_peer
        )

    def t2(b, u, k):
        to = (dev(z, x, 1 - y, c), dev(zat[1], x, y, c), dev(zat[1], x, 1 - y, c))[k]
        there = b ^ 1 if k else b
        return lambda: remote(
            r.s2.at[b, u, k],
            r.r2.at[there, u, k],
            r.t2_send.at[b, u, k],
            r.t2_recv.at[there, u, k],
            to,
        )

    def t3(b, k):
        to = (dev(zat[2], x, y, c), dev(z, 1 - x, y, c), dev(zat[2], 1 - x, y, c))[k]
        return lambda: remote(
            r.s3.at[b, k], r.r3.at[b, k], r.t3_send.at[b, k], r.t3_recv.at[b, k], to
        )

    def compute(b, u):
        part = dot_nn(r.hidden[u], r.w2[zat[b]])
        for zz in range(nz):
            for yy in range(nt // CS):
                at = zz * rows + yy * CS * quarter
                even = part[at : at + quarter]
                odd = part[at + quarter : at + 2 * quarter]
                r.keep[b, u, yy, zz] = jnp.where(low, even, odd)
                r.s1[b, u, yy, zz] = jnp.where(low, odd, even).astype(BF16)
        go(t1(b, u))

    def second(b, u):
        t1(b, u)().wait_recv()

        def value(yy, e):
            return r.keep[b, u, yy, zat[e]] + r.r1[b, u, yy, zat[e]].astype(F32)

        for k, (yy, off) in enumerate(((1 - y, 0), (y, 1), (1 - y, 1))):
            for j in range(2):
                r.s2[b, u, k, j] = value(yy, off ^ (2 * j)).astype(BF16)
            go(t2(b, u, k))
        for e in (0, 2):
            r.keep[b, u, y, zat[e]] = value(y, e)

    def third(b, u):
        for k in range(3):
            t2(b ^ 1 if k else b, u, k)().wait_recv()

        def value(j):
            total = r.keep[b, u, y, zat[2 * j]]
            for k in range(3):
                total += r.r2[b, u, k, j].astype(F32)
            return total

        if u:
            for j in (1, 0):
                r.s3[b, 1 + j] = value(j).astype(BF16)
                go(t3(b, 1 + j))
        else:
            r.s3[b, 0] = value(1).astype(BF16)
            go(t3(b, 0))
            r.acc[zat[b], x] = r.acc[zat[b], x] + value(0)

    def last(b, k):
        t3(b, k)().wait_recv()
        g, v = zat[b if k == 1 else b ^ 2], x if k == 0 else 1 - x
        r.acc[g, v] = r.acc[g, v] + r.r3[b, k].astype(F32)

    def other_hidden():
        for i in range(nz // 2):
            hand_hidden(i)().wait_recv()

    compute(0, 0)
    got_weight(2, 1)
    compute(1, 0)
    second(0, 0)
    second(1, 0)
    got_weight(2, 3)
    compute(3, 0)
    third(0, 0)
    third(1, 0)
    second(3, 0)
    other_hidden()
    compute(0, 1)
    compute(1, 1)
    second(0, 1)
    compute(3, 1)
    second(1, 1)
    got_weight(2, 2)
    compute(2, 0)
    compute(2, 1)
    second(3, 1)
    second(2, 0)
    second(2, 1)
    third(0, 1)
    third(1, 1)
    for b in range(2):
        for k in range(3):
            last(b, k)
    for u in range(XS):
        third(3, u)
        third(2, u)
    for b in range(2, nz):
        for k in range(3):
            last(b, k)
    for g in range(nz):
        for u in range(XS):
            at = g * group + u * width
            r.out[:, at : at + width] = r.acc[g, u].astype(BF16)

    for guard, builds in started.items():

        def drain(builds=builds):
            for build in builds:
                build().wait_send()

        if guard is None:
            drain()
        else:
            pl.when(guards[guard])(drain)


def fast_body(
    queries,
    key_rows,
    value_rows,
    gate_input,
    log_decay,
    head_gain,
    out_weight,
    residual,
    mlp_gain,
    gate_weight,
    up_weight,
    down_weight,
):
    rows, wide = queries.shape
    heads = log_decay.shape[1]
    hd = wide // heads
    model = residual.shape[1]
    ns, nt = lax.axis_size("sp"), lax.axis_size("tp")
    nz = ns // XS
    quarter = rows // nt
    width, units = gate_weight.shape
    share = units // nz
    hh = heads // XS
    vmem = pltpu.VMEM
    dma = pltpu.SemaphoreType.DMA
    operands = {
        "q_hbm": queries,
        "k_hbm": key_rows,
        "v_hbm": value_rows,
        "g_hbm": gate_input,
        "ld_hbm": log_decay.T,
        "hg_hbm": head_gain.reshape(1, wide),
        "res_hbm": residual,
        "mg_hbm": mlp_gain.reshape(1, model),
        "ow_hbm": out_weight,
        "gw_hbm": gate_weight,
        "uw_hbm": up_weight,
        "dw_hbm": down_weight,
    }
    scratch = {
        "q": vmem((rows, wide), BF16),
        "k": vmem((rows, wide), BF16),
        "v": vmem((rows, wide), BF16),
        "g": vmem((rows, wide), BF16),
        "ld": vmem((heads, rows), F32),
        "hg": vmem((1, wide), F32),
        "res": vmem((quarter, model), BF16),
        "mg": vmem((1, model), F32),
        "ow": vmem(out_weight.shape, BF16),
        "raw": vmem((2, width, units), BF16),
        "slab": vmem((3, units, width), BF16),
        "partner": vmem((3, units, width), BF16),
        "wg": vmem((2, ns, share, width), BF16),
        "w2": vmem((nz, share, width), BF16),
        "qrot": vmem((rows, wide), BF16),
        "inner": vmem((rows, wide), F32),
        "cumx": vmem((rows, wide), F32),
        "c_out": vmem((heads, hd, hd), BF16),
        "t_out": vmem((heads, 8, hd), F32),
        "ci": vmem((XS, CS, hh, hd, hd), BF16),
        "ti": vmem((XS, CS, hh, 8, hd), F32),
        "plane": vmem((CS, hh, hd, hd), F32),
        "ch_in": vmem((CS, hh, hd, hd), BF16),
        "ch_out": vmem((CS, hh, hd, hd), BF16),
        "so": vmem((XS, CS, hh, hd, hd), BF16),
        "s_in": vmem((XS, hh, hd, hd), BF16),
        "retained": vmem((rows, wide), BF16),
        "mc_out": vmem((nt // CS, quarter, model), BF16),
        "mc_in": vmem((nt // CS, quarter, model), BF16),
        "mix_own": vmem((nt // CS, quarter, model), F32),
        "my_out": vmem((quarter, model), BF16),
        "my_in": vmem((quarter, model), BF16),
        "acc": vmem((nz, XS, quarter, width), F32),
        "normed": vmem((nz, nt, quarter, model), BF16),
        "gated": vmem((nz // 2, 2 * rows, share), F32),
        "hidden": vmem((XS, nz * rows, share), BF16),
        "keep": vmem((nz, XS, nt // CS, nz, quarter, width), F32),
        "s1": vmem((nz, XS, nt // CS, nz, quarter, width), BF16),
        "r1": vmem((nz, XS, nt // CS, nz, quarter, width), BF16),
        "s2": vmem((nz, XS, 3, 2, quarter, width), BF16),
        "r2": vmem((nz, XS, 3, 2, quarter, width), BF16),
        "s3": vmem((nz, 3, quarter, width), BF16),
        "r3": vmem((nz, 3, quarter, width), BF16),
        "in_sem": dma((len(operands),)),
        "own_sem": dma((3,)),
        "h_send": dma((3,)),
        "h_recv": dma((3,)),
        "w_send": dma((CS, 3, nz)),
        "w_recv": dma((3, nz)),
        "f_send": dma((2, nz)),
        "f_recv": dma((2, nz)),
        "cx_send": dma((2,)),
        "cx_recv": dma((2, CS)),
        "cc_send": dma((2,)),
        "cc_recv": dma((2,)),
        "ch_send": dma,
        "ch_recv": dma,
        "so_send": dma((3,)),
        "s_recv": dma((XS,)),
        "mix_send": dma((2,)),
        "mix_recv": dma((2,)),
        "nc_send": dma,
        "nc_recv": dma,
        "nz_send": dma((3,)),
        "nz_recv": dma((3,)),
        "ny_send": dma((nz,)),
        "ny_recv": dma((nz,)),
        "nd_send": dma((2, nz)),
        "nd_recv": dma((2, nz)),
        "hx_send": dma((nz // 2,)),
        "hx_recv": dma((nz // 2,)),
        "t1_send": dma((nz, XS)),
        "t1_recv": dma((nz, XS)),
        "t2_send": dma((nz, XS, 3)),
        "t2_recv": dma((nz, XS, 3)),
        "t3_send": dma((nz, 3)),
        "t3_recv": dma((nz, 3)),
    }
    names = list(operands) + ["out"] + list(scratch)
    return pl.pallas_call(
        functools.partial(kernel, names, nz, nt),
        out_shape=pltpu.VMEM((quarter, model), BF16),
        in_specs=[pl.BlockSpec(memory_space=pl.ANY)] * len(operands),
        out_specs=pl.BlockSpec(memory_space=pltpu.VMEM),
        scratch_shapes=list(scratch.values()),
        compiler_params=pltpu.CompilerParams(
            collective_id=0, has_side_effects=True, vmem_limit_bytes=60 * 1024 * 1024
        ),
    )(*operands.values())


def fits(mesh, queries, log_decay, gate_weight):
    ns, nt = mesh.shape["sp"], mesh.shape["tp"]
    tokens, wide = queries.shape
    if ns % XS or ns // XS != 4 or nt != 2 * CS or tokens // ns != BLOCK:
        return False
    nz = ns // XS
    hidden = gate_weight.shape[1] // nt
    return (
        gate_weight.shape[0] // ns % 128 == 0
        and hidden % (16 * nz) == 0
        and wide // log_decay.shape[1] == 128
        and BLOCK % (16 * nt) == 0
        and hidden % 128 == 0
        and log_decay.shape[1] // nt % XS == 0
    )


def solution(mesh):
    def run(*args):
        good = fits(mesh, args[0], args[4], args[9])
        return jax.shard_map(
            fast_body if good else body,
            mesh=mesh,
            in_specs=(
                P("sp", "tp"),
                P("sp", "tp"),
                P("sp", "tp"),
                P("sp", "tp"),
                P("sp", "tp"),
                P("tp"),
                P("tp", None),
                P("sp", None),
                P(),
                P("sp", "tp"),
                P("sp", "tp"),
                P("tp", "sp"),
            ),
            out_specs=P(("sp", "tp"), None),
            check_vma=False,
        )(*args)

    return run
```

time: 95.8 us -> 88.7 us (0.926)
  Pallas kernels: 94 us -> 87.9 us
    pallas_call x1, Pallas kernels: 94 us -> 87.9 us  [fast_body(): pl.pallas_call(functools.partial(kernel, names, nz, nt), out_shape=pltpu....]
where the time goes in v1:
time: 88.7 us; the launch traced here: 88.5 us
  Pallas kernels  87.9 us (99%)
    pallas_call x1, Pallas kernels, fast_body(): pl.pallas_call(functools.partial(kernel, names, nz, nt), out_shape=pltpu....  87.9 us

profile of v1, /device:TPU:0, one launch (start us, length us, event | category | flops | bytes accessed | tf_op | source)
XLA Modules:
  0.0 88.5 jit_solution(552224213701630828)
XLA Ops:
  0.0 87.9 %shard_map.118 = bf16[32,2048]{1,0:T(8,128)(2,1)S(1)} custom-call(bf16[128,512]{1,0:T(8,128)(2,1)} %refs_0_.1, bf16[128,512]{1,0:T(8,128)(2,1)} %refs_1_.1, bf16[128,512]{1,0:T(8,128)(2,1)} %refs_2_.1, bf16[128,512]{1,0:T(8,128)(2,1)} %refs_3_.1, f32[4,128]{1,0:T(4,128)} %bitcast.4, f32[1,512]{1,0:T(1,128)} %bitcast.5, bf16[128,2048]{1,0:T(8,128)(2,1)} %refs_6_.1, ...), custom_call_target="tpu_custom_call" | custom-call | tf_op jit(solution)/shard_map/pallas_call | solution.py:881
  87.9 0.7 copy.14

commit v2 on v1

--- a/solution.py
+++ b/solution.py
@@ -194,7 +194,7 @@
 
     barrier = pltpu.get_barrier_semaphore()
     peers = [dev(zat[e], x, y, k) for e in range(1, nz) for k in range(CS)]
-    peers += [c_peer, dev(zat[2], 1 - x, y, c), dev(zat[1], x, 1 - y, c)]
+    peers += [c_peer]
     peers += [dev(z, 1 - x, y, k) for k in range(CS)]
     peers += [dev(z, x, 1 - y, k) for k in range(CS)]
     for peer in peers:
@@ -239,7 +239,7 @@
         return ref.at[m, pl.ds(pl.multiple_of(zz * share, 16), share)]
 
     def slot(m, zz):
-        return r.w2.at[zz] if m == 2 else r.wg.at[m, zz * XS + x]
+        return r.wg.at[m, zz * XS + x]
 
     own_copies = {}
 
@@ -277,7 +277,8 @@
         weight(m, e, k) for m in range(3) for e in range(1, nz) for k in range(CS)
     ]
     outer = jnp.logical_or(z == 0, z == nz - 1)
-    outer_plan = ((0, 1), (1, 1), (0, 2), (0, 3), (2, 1), (1, 2), (1, 3))
+    outer_head = ((0, 1), (1, 1))
+    outer_tail = ((2, 1), (0, 2), (0, 3), (1, 2), (1, 3))
     inner_head = ((0, 3), (0, 1), (1, 3), (1, 1))
     inner_tail = ((0, 2), (2, 1), (1, 2))
 
@@ -299,10 +300,24 @@
             got_weight(m, e)
         go(forward(m, e))
 
+    def pass_if(when, pieces):
+        @pl.when(when)
+        def _():
+            for m, e in pieces:
+                got_weight(m, e)
+                forward(m, e)().start()
+
+    near = ((0, 1), (1, 1))
+    started[None] = [forward(m, e) for m, e in near + ((0, 3),)]
+
     @pl.when(c == 1)
     def _():
         for m in range(3):
             go(hand(m), "c1")
+
+    @pl.when(jnp.logical_and(c == 0, outer))
+    def _():
+        send_weights(outer_head, (0,))
 
     @pl.when(jnp.logical_and(c == 0, jnp.logical_not(outer)))
     def _():
@@ -394,7 +409,8 @@
 
         @pl.when(outer)
         def _():
-            send_weights(outer_plan)
+            send_weights(outer_head, (1,))
+            send_weights(outer_tail)
 
         @pl.when(jnp.logical_not(outer))
         def _():
@@ -404,6 +420,7 @@
     pass_on(0, 0)
     pass_on(1, 0)
     first = x == 0
+    late = z >= nz // 2
 
     @pl.when(c == 1)
     def _():
@@ -423,6 +440,8 @@
                 late_t = jnp.where(first, other_t, own_t)
                 r.plane[k, i] = late_t * early_c + late_c
 
+        pass_if(late, near)
+
         @pl.when(z == 0)
         def _():
             r.ch_in[...] = jnp.zeros(r.ch_in.shape, BF16)
@@ -456,8 +475,11 @@
 
     @pl.when(c == 0)
     def _():
+        pass_if(late, near)
         state_c().wait_recv()
 
+    own_copies[2].wait()
+    pass_on(2, 0)
     state_x(0)().wait_recv()
     loads["g"].wait()
     loads["hg"].wait()
@@ -494,7 +516,10 @@
     mix_c().wait_recv()
     r.my_out[...] = (r.mix_own[1 - y] + r.mc_in[1 - y].astype(F32)).astype(BF16)
     go(mix_y)
-    pass_on(0, 1)
+    early = jnp.logical_not(late)
+    pass_if(early, near)
+    pass_on(0, 2)
+    pass_if(late, ((0, 3),))
     mixed = r.mix_own[y] + r.mc_in[y].astype(F32)
     mix_y().wait_recv()
     mixed += r.my_in[...].astype(F32)
@@ -513,60 +538,39 @@
         rows_at = r.normed.at[z, tp]
         return remote(rows_at, rows_at, r.nc_send, r.nc_recv, c_peer)
 
-    def pair(zz, yy):
-        return r.normed.at[zz, pl.ds(yy * CS, CS)]
-
-    def rows_z(k):
+    def rows_of(zz, yy, j):
+        return r.normed.at[zz, yy * CS + j]
+
+    def rows_z(k, j):
         to = zat[2] if k == 0 else zat[1]
         zz = zat[2] if k == 2 else z
         return lambda: remote(
-            pair(zz, y), pair(zz, y), r.nz_send.at[k], r.nz_recv.at[k], dev(to, x, y, 1)
-        )
-
-    def rows_y(e):
+            rows_of(zz, y, j),
+            rows_of(zz, y, j),
+            r.nz_send.at[k, j],
+            r.nz_recv.at[k, j],
+            dev(to, x, y, 1),
+        )
+
+    def rows_y(e, j):
         return lambda: remote(
-            pair(zat[e], y),
-            pair(zat[e], y),
-            r.ny_send.at[e],
-            r.ny_recv.at[e],
+            rows_of(zat[e], y, j),
+            rows_of(zat[e], y, j),
+            r.ny_send.at[e, j],
+            r.ny_recv.at[e, j],
             dev(z, x, 1 - y, 1),
         )
 
-    def rows_d(e, v):
+    def rows_d(e, v, j):
         def build():
-            rows_at = pair(zat[e], 1 - y if v else y)
+            rows_at = rows_of(zat[e], 1 - y if v else y, j)
             return remote(
-                rows_at, rows_at, r.nd_send.at[v, e], r.nd_recv.at[v, e], dev(z, x, y, 0)
+                rows_at, rows_at, r.nd_send.at[v, e, j], r.nd_recv.at[v, e, j], dev(z, x, y, 0)
             )
 
         return build
 
     go(rows_c)
-    rows_c().wait_recv()
-
-    @pl.when(c == 1)
-    def _():
-        for k in range(2):
-            go(rows_z(k), "c1")
-        go(rows_y(0), "c1")
-
-    pass_on(1, 1)
-    pass_on(0, 2)
-
-    @pl.when(c == 1)
-    def _():
-        rows_z(1)().wait_recv()
-        go(rows_y(1), "c1")
-        go(rows_d(1, 0), "c1")
-        rows_y(0)().wait_recv()
-        go(rows_d(0, 1), "c1")
-        rows_z(0)().wait_recv()
-        go(rows_z(2), "c1")
-        go(rows_y(2), "c1")
-        go(rows_d(2, 0), "c1")
-
-    pass_on(0, 3)
-    pass_on(1, 3)
 
     def send_down(if_outer, if_inner):
         @pl.when(outer)
@@ -579,58 +583,104 @@
 
     @pl.when(c == 1)
     def _():
-        rows_y(1)().wait_recv()
-        go(rows_d(1, 1), "c1")
-        rows_z(2)().wait_recv()
-        go(rows_y(3), "c1")
-        go(rows_d(3, 0), "c1")
-        rows_y(2)().wait_recv()
-        go(rows_d(2, 1), "c1")
-        rows_y(3)().wait_recv()
-        go(rows_d(3, 1), "c1")
+        for j in (1, 0):
+            if j == 0:
+                rows_c().wait_recv()
+            for k in range(2):
+                go(rows_z(k, j), "c1")
+            go(rows_y(0, j), "c1")
 
     @pl.when(c == 0)
     def _():
-        rows_d(2, 0)().wait_recv()
+        rows_c().wait_recv()
+
+    pass_if(early, ((0, 3),))
+    pass_on(2, 1)
+    pass_on(1, 3)
+
+    @pl.when(c == 1)
+    def _():
+        for j in (1, 0):
+            rows_z(1, j)().wait_recv()
+            go(rows_y(1, j), "c1")
+            go(rows_d(1, 0, j), "c1")
+        for j in (1, 0):
+            rows_y(0, j)().wait_recv()
+            go(rows_d(0, 1, j), "c1")
+        for j in (1, 0):
+            rows_z(0, j)().wait_recv()
+            go(rows_z(2, j), "c1")
+            go(rows_y(2, j), "c1")
+            go(rows_d(2, 0, j), "c1")
+
+    pass_on(1, 2)
+
+    @pl.when(c == 0)
+    def _():
+        for j in (1, 0):
+            rows_d(2, 0, j)().wait_recv()
         send_down(2, 3)
 
-    pass_on(1, 2)
+    @pl.when(c == 1)
+    def _():
+        for j in (1, 0):
+            rows_y(1, j)().wait_recv()
+            go(rows_d(1, 1, j), "c1")
+        for j in (1, 0):
+            rows_z(2, j)().wait_recv()
+            go(rows_y(3, j), "c1")
+            go(rows_d(3, 0, j), "c1")
 
     @pl.when(c == 0)
     def _():
-        rows_d(3, 0)().wait_recv()
+        for j in (1, 0):
+            rows_d(3, 0, j)().wait_recv()
         send_down(3, 2)
-        rows_d(1, 0)().wait_recv()
-        for e in range(nz):
-            rows_d(e, 1)().wait_recv()
-
-    def project(m, lo, hi):
-        block = r.normed[lo:hi].reshape((hi - lo) * rows, r.normed.shape[3])
+        for e, v in ((1, 0), (0, 1), (1, 1)):
+            for j in (1, 0):
+                rows_d(e, v, j)().wait_recv()
+
+    def project(m, half_z):
+        block = r.normed[pl.ds(2 * half_z, 2)].reshape(2 * rows, r.normed.shape[3])
         total = dot_nt(block[:, :width], r.wg[m, 0])
         for s in range(1, ns):
             total += dot_nt(block[:, s * width : (s + 1) * width], r.wg[m, s])
         return total
 
-    def hand_hidden(i):
-        at = pl.ds(i * 2 * rows, 2 * rows)
-        return lambda: remote(
-            r.hidden.at[0, at], r.hidden.at[1, at], r.hx_send.at[i], r.hx_recv.at[i], x_peer
-        )
-
+    def gate_rows(half_z):
+        gate = project(0, half_z)
+        r.gated[half_z] = gate / (1.0 + jnp.exp(-gate))
+
+    def up_rows(half_z):
+        at = pl.ds(pl.multiple_of(half_z * 2 * rows, 2 * rows), 2 * rows)
+        r.hidden[at, :] = (r.gated[half_z] * project(1, half_z)).astype(BF16)
+
+    own_half = z // 2
     own_copies[0].wait()
     for e in range(nz):
         forward(0, e)().wait_recv()
-    for i in range(nz // 2):
-        gate = project(0, 2 * i, 2 * i + 2)
-        r.gated[i] = gate / (1.0 + jnp.exp(-gate))
+    gate_rows(own_half)
+
+    @pl.when(c == 1)
+    def _():
+        for e in (2, 3):
+            for j in (1, 0):
+                rows_y(e, j)().wait_recv()
+                go(rows_d(e, 1, j), "c1")
+
     own_copies[1].wait()
     for e in range(nz):
         forward(1, e)().wait_recv()
-    for i in range(nz // 2):
-        at = slice(i * 2 * rows, (i + 1) * 2 * rows)
-        r.hidden[0, at, :] = (r.gated[i] * project(1, 2 * i, 2 * i + 2)).astype(BF16)
-        go(hand_hidden(i))
-    own_copies[2].wait()
+    up_rows(own_half)
+
+    @pl.when(c == 0)
+    def _():
+        for e in (2, 3):
+            for j in (1, 0):
+                rows_d(e, 1, j)().wait_recv()
+
+    gate_rows(1 - own_half)
+    up_rows(1 - own_half)
 
     low = c == 0
 
@@ -639,25 +689,31 @@
             r.s1.at[b, u], r.r1.at[b, u], r.t1_send.at[b, u], r.t1_recv.at[b, u], c_peer
         )
 
-    def t2(b, u, k):
-        to = (dev(z, x, 1 - y, c), dev(zat[1], x, y, c), dev(zat[1], x, 1 - y, c))[k]
-        there = b ^ 1 if k else b
+    def t2(b, u):
         return lambda: remote(
-            r.s2.at[b, u, k],
-            r.r2.at[there, u, k],
-            r.t2_send.at[b, u, k],
-            r.t2_recv.at[there, u, k],
-            to,
-        )
-
-    def t3(b, k):
-        to = (dev(zat[2], x, y, c), dev(z, 1 - x, y, c), dev(zat[2], 1 - x, y, c))[k]
+            r.s2.at[b, u],
+            r.r2.at[b, u],
+            r.t2_send.at[b, u],
+            r.t2_recv.at[b, u],
+            dev(z, x, 1 - y, c),
+        )
+
+    def t3(b, u, e):
         return lambda: remote(
-            r.s3.at[b, k], r.r3.at[b, k], r.t3_send.at[b, k], r.t3_recv.at[b, k], to
-        )
+            r.s3.at[b, u, e],
+            r.r3.at[b, u, e],
+            r.t3_send.at[b, u, e],
+            r.t3_recv.at[b, u, e],
+            dev(zat[e], x, y, c),
+        )
+
+    def side(u):
+        return 1 - x if u else x
 
     def compute(b, u):
-        part = dot_nn(r.hidden[u], r.w2[zat[b]])
+        if u:
+            forward(2, b)().wait_recv()
+        part = dot_nn(r.hidden[...], r.wg[2, zat[b] * XS + side(u)])
         for zz in range(nz):
             for yy in range(nt // CS):
                 at = zz * rows + yy * CS * quarter
@@ -669,78 +725,52 @@
 
     def second(b, u):
         t1(b, u)().wait_recv()
-
-        def value(yy, e):
-            return r.keep[b, u, yy, zat[e]] + r.r1[b, u, yy, zat[e]].astype(F32)
-
-        for k, (yy, off) in enumerate(((1 - y, 0), (y, 1), (1 - y, 1))):
-            for j in range(2):
-                r.s2[b, u, k, j] = value(yy, off ^ (2 * j)).astype(BF16)
-            go(t2(b, u, k))
-        for e in (0, 2):
-            r.keep[b, u, y, zat[e]] = value(y, e)
+        r.s2[b, u] = (r.keep[b, u, 1 - y] + r.r1[b, u, 1 - y].astype(F32)).astype(BF16)
+        go(t2(b, u))
+        r.keep[b, u, y] = r.keep[b, u, y] + r.r1[b, u, y].astype(F32)
 
     def third(b, u):
-        for k in range(3):
-            t2(b ^ 1 if k else b, u, k)().wait_recv()
-
-        def value(j):
-            total = r.keep[b, u, y, zat[2 * j]]
-            for k in range(3):
-                total += r.r2[b, u, k, j].astype(F32)
-            return total
-
-        if u:
-            for j in (1, 0):
-                r.s3[b, 1 + j] = value(j).astype(BF16)
-                go(t3(b, 1 + j))
-        else:
-            r.s3[b, 0] = value(1).astype(BF16)
-            go(t3(b, 0))
-            r.acc[zat[b], x] = r.acc[zat[b], x] + value(0)
-
-    def last(b, k):
-        t3(b, k)().wait_recv()
-        g, v = zat[b if k == 1 else b ^ 2], x if k == 0 else 1 - x
-        r.acc[g, v] = r.acc[g, v] + r.r3[b, k].astype(F32)
-
-    def other_hidden():
-        for i in range(nz // 2):
-            hand_hidden(i)().wait_recv()
-
-    compute(0, 0)
-    got_weight(2, 1)
-    compute(1, 0)
-    second(0, 0)
-    second(1, 0)
-    got_weight(2, 3)
+        t2(b, u)().wait_recv()
+        for e in (3, 2, 1):
+            total = r.keep[b, u, y, zat[e]] + r.r2[b, u, zat[e]].astype(F32)
+            r.s3[b, u, e] = total.astype(BF16)
+            go(t3(b, u, e))
+        total = r.keep[b, u, y, z] + r.r2[b, u, z].astype(F32)
+        r.acc[zat[b], side(u)] = r.acc[zat[b], side(u)] + total
+
+    def last(b, u):
+        for e in (1, 3, 2):
+            t3(b, u, e)().wait_recv()
+            g = zat[b ^ e]
+            r.acc[g, side(u)] = r.acc[g, side(u)] + r.r3[b, u, e].astype(F32)
+
+    for b in range(2):
+        for u in range(XS):
+            compute(b, u)
+    for b in range(2):
+        for u in range(XS):
+            second(b, u)
+    pass_on(2, 3)
     compute(3, 0)
     third(0, 0)
+    third(0, 1)
+    pass_on(2, 2)
+    compute(2, 0)
+    second(3, 0)
     third(1, 0)
-    second(3, 0)
-    other_hidden()
-    compute(0, 1)
-    compute(1, 1)
-    second(0, 1)
+    third(1, 1)
+    second(2, 0)
     compute(3, 1)
-    second(1, 1)
-    got_weight(2, 2)
-    compute(2, 0)
+    second(3, 1)
     compute(2, 1)
-    second(3, 1)
-    second(2, 0)
     second(2, 1)
-    third(0, 1)
-    third(1, 1)
-    for b in range(2):
-        for k in range(3):
-            last(b, k)
-    for u in range(XS):
-        third(3, u)
-        third(2, u)
-    for b in range(2, nz):
-        for k in range(3):
-            last(b, k)
+    for b, u in ((3, 0), (2, 0), (3, 1), (2, 1)):
+        third(b, u)
+    for b in (0, 1):
+        for u in range(XS):
+            last(b, u)
+    for b, u in ((3, 0), (2, 0), (3, 1), (2, 1)):
+        last(b, u)
     for g in range(nz):
         for u in range(XS):
             at = g * group + u * width
@@ -811,8 +841,7 @@
         "raw": vmem((2, width, units), BF16),
         "slab": vmem((3, units, width), BF16),
         "partner": vmem((3, units, width), BF16),
-        "wg": vmem((2, ns, share, width), BF16),
-        "w2": vmem((nz, share, width), BF16),
+        "wg": vmem((3, ns, share, width), BF16),
         "qrot": vmem((rows, wide), BF16),
         "inner": vmem((rows, wide), F32),
         "cumx": vmem((rows, wide), F32),
@@ -834,22 +863,22 @@
         "acc": vmem((nz, XS, quarter, width), F32),
         "normed": vmem((nz, nt, quarter, model), BF16),
         "gated": vmem((nz // 2, 2 * rows, share), F32),
-        "hidden": vmem((XS, nz * rows, share), BF16),
+        "hidden": vmem((nz * rows, share), BF16),
         "keep": vmem((nz, XS, nt // CS, nz, quarter, width), F32),
         "s1": vmem((nz, XS, nt // CS, nz, quarter, width), BF16),
         "r1": vmem((nz, XS, nt // CS, nz, quarter, width), BF16),
-        "s2": vmem((nz, XS, 3, 2, quarter, width), BF16),
-        "r2": vmem((nz, XS, 3, 2, quarter, width), BF16),
-        "s3": vmem((nz, 3, quarter, width), BF16),
-        "r3": vmem((nz, 3, quarter, width), BF16),
+        "s2": vmem((nz, XS, nz, quarter, width), BF16),
+        "r2": vmem((nz, XS, nz, quarter, width), BF16),
+        "s3": vmem((nz, XS, nz, quarter, width), BF16),
+        "r3": vmem((nz, XS, nz, quarter, width), BF16),
         "in_sem": dma((len(operands),)),
         "own_sem": dma((3,)),
         "h_send": dma((3,)),
         "h_recv": dma((3,)),
         "w_send": dma((CS, 3, nz)),
         "w_recv": dma((3, nz)),
-        "f_send": dma((2, nz)),
-        "f_recv": dma((2, nz)),
+        "f_send": dma((3, nz)),
+        "f_recv": dma((3, nz)),
         "cx_send": dma((2,)),
         "cx_recv": dma((2, CS)),
         "cc_send": dma((2,)),
@@ -862,20 +891,18 @@
         "mix_recv": dma((2,)),
         "nc_send": dma,
         "nc_recv": dma,
-        "nz_send": dma((3,)),
-        "nz_recv": dma((3,)),
-        "ny_send": dma((nz,)),
-        "ny_recv": dma((nz,)),
-        "nd_send": dma((2, nz)),
-        "nd_recv": dma((2, nz)),
-        "hx_send": dma((nz // 2,)),
-        "hx_recv": dma((nz // 2,)),
+        "nz_send": dma((3, CS)),
+        "nz_recv": dma((3, CS)),
+        "ny_send": dma((nz, CS)),
+        "ny_recv": dma((nz, CS)),
+        "nd_send": dma((2, nz, CS)),
+        "nd_recv": dma((2, nz, CS)),
         "t1_send": dma((nz, XS)),
         "t1_recv": dma((nz, XS)),
-        "t2_send": dma((nz, XS, 3)),
-        "t2_recv": dma((nz, XS, 3)),
-        "t3_send": dma((nz, 3)),
-        "t3_recv": dma((nz, 3)),
+        "t2_send": dma((nz, XS)),
+        "t2_recv": dma((nz, XS)),
+        "t3_send": dma((nz, XS, nz)),
+        "t3_recv": dma((nz, XS, nz)),
     }
     names = list(operands) + ["out"] + list(scratch)
     return pl.pallas_call(

time: 88.7 us -> 81 us (0.913)
  Pallas kernels: 87.9 us -> 80.1 us
    pallas_call x1, Pallas kernels: 87.9 us -> 80.1 us  [fast_body(): pl.pallas_call(functools.partial(kernel, names, nz, nt), out_shape=pltpu....]
where the time goes in v2:
time: 81 us; the launch traced here: 80.8 us
  Pallas kernels  80.1 us (99%)
    pallas_call x1, Pallas kernels, fast_body(): pl.pallas_call(functools.partial(kernel, names, nz, nt), out_shape=pltpu....  80.1 us

profile of v2, /device:TPU:0, one launch (start us, length us, event | category | flops | bytes accessed | tf_op | source)
XLA Modules:
  0.0 80.8 jit_solution(17284275511978935930)
XLA Ops:
  0.0 80.1 %shard_map.118 = bf16[32,2048]{1,0:T(8,128)(2,1)S(1)} custom-call(bf16[128,512]{1,0:T(8,128)(2,1)} %refs_0_.1, bf16[128,512]{1,0:T(8,128)(2,1)} %refs_1_.1, bf16[128,512]{1,0:T(8,128)(2,1)} %refs_2_.1, bf16[128,512]{1,0:T(8,128)(2,1)} %refs_3_.1, f32[4,128]{1,0:T(4,128)} %bitcast.4, f32[1,512]{1,0:T(1,128)} %bitcast.5, bf16[128,2048]{1,0:T(8,128)(2,1)} %refs_6_.1, ...), custom_call_target="tpu_custom_call" | custom-call | tf_op jit(solution)/shard_map/pallas_call | solution.py:908
  80.2 0.7 copy.14

commit v3 on v2

--- a/solution.py
+++ b/solution.py
@@ -194,7 +194,7 @@
 
     barrier = pltpu.get_barrier_semaphore()
     peers = [dev(zat[e], x, y, k) for e in range(1, nz) for k in range(CS)]
-    peers += [c_peer]
+    peers += [c_peer] + [dev(zat[e], 1 - x, y, c) for e in range(1, nz)]
     peers += [dev(z, 1 - x, y, k) for k in range(CS)]
     peers += [dev(z, x, 1 - y, k) for k in range(CS)]
     for peer in peers:
@@ -226,14 +226,11 @@
             device_id_type=MESH,
         )
 
-    started = {}
-
-    def go(build, guard=None):
+    def go(build):
         build().start()
-        started.setdefault(guard, []).append(build)
-        return build
-
-    guards = {"c0": c == 0, "c1": c == 1, "up": jnp.logical_and(c == 1, z < nz - 1)}
+
+    def sent(view, sem):
+        remote(view, view, sem, sem, c_peer).wait_send()
 
     def piece(ref, m, zz):
         return ref.at[m, pl.ds(pl.multiple_of(zz * share, 16), share)]
@@ -260,7 +257,7 @@
 
     def hand(m):
         return lambda: remote(
-            r.slab.at[m], r.partner.at[m], r.h_send.at[m], r.h_recv.at[m], c_peer
+            r.slab.at[m], r.partner.at[m], r.h_send, r.h_recv.at[m], c_peer
         )
 
     def weight(m, e, k):
@@ -268,14 +265,11 @@
         return lambda: remote(
             piece(source, m, zat[e]),
             slot(m, z),
-            r.w_send.at[k, m, e],
-            r.w_recv.at[m, e],
+            r.w_send,
+            r.w_recv.at[m, e - 1],
             dev(zat[e], x, y, k),
         )
 
-    started["c0"] = [
-        weight(m, e, k) for m in range(3) for e in range(1, nz) for k in range(CS)
-    ]
     outer = jnp.logical_or(z == 0, z == nz - 1)
     outer_head = ((0, 1), (1, 1))
     outer_tail = ((2, 1), (0, 2), (0, 3), (1, 2), (1, 3))
@@ -293,7 +287,8 @@
     def forward(m, e):
         at = slot(m, zat[e])
         source = piece(r.slab, m, z) if e == 0 else at
-        return lambda: remote(source, at, r.f_send.at[m, e], r.f_recv.at[m, e], x_peer)
+        recv = r.f_recv.at[2 + e] if m == 2 else r.f_recv.at[m]
+        return lambda: remote(source, at, r.f_send, recv, x_peer)
 
     def pass_on(m, e):
         if e:
@@ -308,12 +303,15 @@
                 forward(m, e)().start()
 
     near = ((0, 1), (1, 1))
-    started[None] = [forward(m, e) for m, e in near + ((0, 3),)]
+
+    def got_forwards(m):
+        view = r.wg.at[m, :nz]
+        remote(view, view, r.f_send, r.f_recv.at[m], x_peer).wait_recv()
 
     @pl.when(c == 1)
     def _():
         for m in range(3):
-            go(hand(m), "c1")
+            go(hand(m))
 
     @pl.when(jnp.logical_and(c == 0, outer))
     def _():
@@ -402,8 +400,8 @@
 
     @pl.when(c == 0)
     def _():
-        go(near_c, "c0")
-        go(near_t, "c0")
+        go(near_c)
+        go(near_t)
         for m in range(3):
             hand(m)().wait_recv()
 
@@ -417,10 +415,16 @@
             send_weights(inner_head, (1,))
             send_weights(inner_tail)
 
-    pass_on(0, 0)
-    pass_on(1, 0)
+    late = z >= nz // 2
     first = x == 0
-    late = z >= nz // 2
+
+    def pass_own(when):
+        @pl.when(when)
+        def _():
+            for m in range(2):
+                forward(m, 0)().start()
+
+    pass_own(late)
 
     @pl.when(c == 1)
     def _():
@@ -458,7 +462,7 @@
 
         @pl.when(z < nz - 1)
         def _():
-            go(chain, "up")
+            go(chain)
 
         for k in range(CS):
             for i in range(hh):
@@ -469,8 +473,8 @@
                 r.so[0, k, i] = jnp.where(first, state, after).astype(BF16)
                 r.so[1, k, i] = jnp.where(first, after, state).astype(BF16)
         for k in range(CS):
-            go(state_x(k), "c1")
-        go(state_c, "c1")
+            go(state_x(k))
+        go(state_c)
         r.s_in[0] = r.so[0, 1]
 
     @pl.when(c == 0)
@@ -478,8 +482,7 @@
         pass_if(late, near)
         state_c().wait_recv()
 
-    own_copies[2].wait()
-    pass_on(2, 0)
+    pass_own(jnp.logical_not(late))
     state_x(0)().wait_recv()
     loads["g"].wait()
     loads["hg"].wait()
@@ -547,7 +550,7 @@
         return lambda: remote(
             rows_of(zz, y, j),
             rows_of(zz, y, j),
-            r.nz_send.at[k, j],
+            r.nz_send,
             r.nz_recv.at[k, j],
             dev(to, x, y, 1),
         )
@@ -556,7 +559,7 @@
         return lambda: remote(
             rows_of(zat[e], y, j),
             rows_of(zat[e], y, j),
-            r.ny_send.at[e, j],
+            r.ny_send,
             r.ny_recv.at[e, j],
             dev(z, x, 1 - y, 1),
         )
@@ -565,10 +568,14 @@
         def build():
             rows_at = rows_of(zat[e], 1 - y if v else y, j)
             return remote(
-                rows_at, rows_at, r.nd_send.at[v, e, j], r.nd_recv.at[v, e, j], dev(z, x, y, 0)
+                rows_at, rows_at, r.nd_send.at[v], r.nd_recv.at[v, e], dev(z, x, y, 0)
             )
 
         return build
+
+    def got_rows(e, v):
+        view = r.normed.at[zat[e], pl.ds((1 - y if v else y) * CS, CS)]
+        remote(view, view, r.nd_send.at[v], r.nd_recv.at[v, e], c_peer).wait_recv()
 
     go(rows_c)
 
@@ -587,58 +594,57 @@
             if j == 0:
                 rows_c().wait_recv()
             for k in range(2):
-                go(rows_z(k, j), "c1")
-            go(rows_y(0, j), "c1")
+                go(rows_z(k, j))
+            go(rows_y(0, j))
 
     @pl.when(c == 0)
     def _():
         rows_c().wait_recv()
 
     pass_if(early, ((0, 3),))
-    pass_on(2, 1)
+    own_copies[2].wait()
+    pass_on(2, 0)
     pass_on(1, 3)
 
     @pl.when(c == 1)
     def _():
         for j in (1, 0):
             rows_z(1, j)().wait_recv()
-            go(rows_y(1, j), "c1")
-            go(rows_d(1, 0, j), "c1")
+            go(rows_y(1, j))
+            go(rows_d(1, 0, j))
         for j in (1, 0):
             rows_y(0, j)().wait_recv()
-            go(rows_d(0, 1, j), "c1")
+            go(rows_d(0, 1, j))
         for j in (1, 0):
             rows_z(0, j)().wait_recv()
-            go(rows_z(2, j), "c1")
-            go(rows_y(2, j), "c1")
-            go(rows_d(2, 0, j), "c1")
+            go(rows_z(2, j))
+            go(rows_y(2, j))
+            go(rows_d(2, 0, j))
 
     pass_on(1, 2)
+    pass_on(2, 1)
 
     @pl.when(c == 0)
     def _():
-        for j in (1, 0):
-            rows_d(2, 0, j)().wait_recv()
+        got_rows(2, 0)
         send_down(2, 3)
 
     @pl.when(c == 1)
     def _():
         for j in (1, 0):
             rows_y(1, j)().wait_recv()
-            go(rows_d(1, 1, j), "c1")
+            go(rows_d(1, 1, j))
         for j in (1, 0):
             rows_z(2, j)().wait_recv()
-            go(rows_y(3, j), "c1")
-            go(rows_d(3, 0, j), "c1")
+            go(rows_y(3, j))
+            go(rows_d(3, 0, j))
 
     @pl.when(c == 0)
     def _():
-        for j in (1, 0):
-            rows_d(3, 0, j)().wait_recv()
+        got_rows(3, 0)
         send_down(3, 2)
         for e, v in ((1, 0), (0, 1), (1, 1)):
-            for j in (1, 0):
-                rows_d(e, v, j)().wait_recv()
+            got_rows(e, v)
 
     def project(m, half_z):
         block = r.normed[pl.ds(2 * half_z, 2)].reshape(2 * rows, r.normed.shape[3])
@@ -651,14 +657,23 @@
         gate = project(0, half_z)
         r.gated[half_z] = gate / (1.0 + jnp.exp(-gate))
 
-    def up_rows(half_z):
-        at = pl.ds(pl.multiple_of(half_z * 2 * rows, 2 * rows), 2 * rows)
-        r.hidden[at, :] = (r.gated[half_z] * project(1, half_z)).astype(BF16)
+    def half_at(half_z):
+        return pl.ds(pl.multiple_of(half_z * 2 * rows, 2 * rows), 2 * rows)
+
+    def hand_hidden(i):
+        at = half_at(own_half if i == 0 else 1 - own_half)
+        return lambda: remote(
+            r.hidden.at[0, at], r.hidden.at[1, at], r.hx_send, r.hx_recv.at[i], x_peer
+        )
+
+    def up_rows(i):
+        half_z = own_half if i == 0 else 1 - own_half
+        r.hidden[0, half_at(half_z), :] = (r.gated[half_z] * project(1, half_z)).astype(BF16)
+        go(hand_hidden(i))
 
     own_half = z // 2
     own_copies[0].wait()
-    for e in range(nz):
-        forward(0, e)().wait_recv()
+    got_forwards(0)
     gate_rows(own_half)
 
     @pl.when(c == 1)
@@ -666,44 +681,53 @@
         for e in (2, 3):
             for j in (1, 0):
                 rows_y(e, j)().wait_recv()
-                go(rows_d(e, 1, j), "c1")
+                go(rows_d(e, 1, j))
 
     own_copies[1].wait()
-    for e in range(nz):
-        forward(1, e)().wait_recv()
-    up_rows(own_half)
+    got_forwards(1)
+    up_rows(0)
 
     @pl.when(c == 0)
     def _():
         for e in (2, 3):
-            for j in (1, 0):
-                rows_d(e, 1, j)().wait_recv()
+            got_rows(e, 1)
 
     gate_rows(1 - own_half)
-    up_rows(1 - own_half)
+    up_rows(1)
 
     low = c == 0
 
     def t1(b, u):
         return lambda: remote(
-            r.s1.at[b, u], r.r1.at[b, u], r.t1_send.at[b, u], r.t1_recv.at[b, u], c_peer
+            r.s1.at[b, u], r.r1.at[b, u], r.t1_send, r.t1_recv.at[b, u], c_peer
         )
 
     def t2(b, u):
         return lambda: remote(
             r.s2.at[b, u],
             r.r2.at[b, u],
-            r.t2_send.at[b, u],
+            r.t2_send,
             r.t2_recv.at[b, u],
             dev(z, x, 1 - y, c),
         )
 
+    def unit(b, u):
+        return XS * b + u if b < 2 else b + 2
+
     def t3(b, u, e):
+        if b > 1 and u:
+            return lambda: remote(
+                r.s3x.at[b - 2, e],
+                r.r3x.at[b - 2, e],
+                r.t3x_send,
+                r.t3x_recv.at[b - 2],
+                dev(zat[e], 1 - x, y, c),
+            )
         return lambda: remote(
-            r.s3.at[b, u, e],
-            r.r3.at[b, u, e],
-            r.t3_send.at[b, u, e],
-            r.t3_recv.at[b, u, e],
+            r.s3.at[unit(b, u), e - 1],
+            r.r3.at[unit(b, u), e - 1],
+            r.t3_send,
+            r.t3_recv.at[unit(b, u)],
             dev(zat[e], x, y, c),
         )
 
@@ -711,9 +735,12 @@
         return 1 - x if u else x
 
     def compute(b, u):
-        if u:
-            forward(2, b)().wait_recv()
-        part = dot_nn(r.hidden[...], r.wg[2, zat[b] * XS + side(u)])
+        if b < 2:
+            if u:
+                forward(2, b)().wait_recv()
+            part = dot_nn(r.hidden[0], r.wg[2, zat[b] * XS + side(u)])
+        else:
+            part = dot_nn(r.hidden[u], r.wg[2, zat[b] * XS + x])
         for zz in range(nz):
             for yy in range(nt // CS):
                 at = zz * rows + yy * CS * quarter
@@ -731,18 +758,36 @@
 
     def third(b, u):
         t2(b, u)().wait_recv()
+        def value(e):
+            return r.keep[b, u, y, zat[e]] + r.r2[b, u, zat[e]].astype(F32)
+
+        if b > 1 and u:
+            for e in (3, 2, 1, 0):
+                r.s3x[b - 2, e] = value(e).astype(BF16)
+                go(t3(b, u, e))
+            return
         for e in (3, 2, 1):
-            total = r.keep[b, u, y, zat[e]] + r.r2[b, u, zat[e]].astype(F32)
-            r.s3[b, u, e] = total.astype(BF16)
+            r.s3[unit(b, u), e - 1] = value(e).astype(BF16)
             go(t3(b, u, e))
-        total = r.keep[b, u, y, z] + r.r2[b, u, z].astype(F32)
-        r.acc[zat[b], side(u)] = r.acc[zat[b], side(u)] + total
+        r.acc[zat[b], side(u)] = r.acc[zat[b], side(u)] + value(0)
 
     def last(b, u):
+        if b > 1 and u:
+            view = r.r3x.at[b - 2]
+            remote(view, view, r.t3x_send, r.t3x_recv.at[b - 2], c_peer).wait_recv()
+            for e in range(nz):
+                g = zat[b ^ e]
+                r.acc[g, 1 - x] = r.acc[g, 1 - x] + r.r3x[b - 2, e].astype(F32)
+            return
+        view = r.r3.at[unit(b, u)]
+        remote(view, view, r.t3_send, r.t3_recv.at[unit(b, u)], c_peer).wait_recv()
         for e in (1, 3, 2):
-            t3(b, u, e)().wait_recv()
             g = zat[b ^ e]
-            r.acc[g, side(u)] = r.acc[g, side(u)] + r.r3[b, u, e].astype(F32)
+            r.acc[g, side(u)] = r.acc[g, side(u)] + r.r3[unit(b, u), e - 1].astype(F32)
+
+    def other_hidden():
+        for i in range(2):
+            hand_hidden(i)().wait_recv()
 
     for b in range(2):
         for u in range(XS):
@@ -750,22 +795,25 @@
     for b in range(2):
         for u in range(XS):
             second(b, u)
-    pass_on(2, 3)
+    got_weight(2, 3)
     compute(3, 0)
     third(0, 0)
     third(0, 1)
-    pass_on(2, 2)
-    compute(2, 0)
     second(3, 0)
     third(1, 0)
+    got_weight(2, 2)
+    compute(2, 0)
+    other_hidden()
+    compute(3, 1)
+    compute(2, 1)
     third(1, 1)
     second(2, 0)
-    compute(3, 1)
     second(3, 1)
-    compute(2, 1)
     second(2, 1)
-    for b, u in ((3, 0), (2, 0), (3, 1), (2, 1)):
-        third(b, u)
+    third(3, 0)
+    third(2, 0)
+    third(3, 1)
+    third(2, 1)
     for b in (0, 1):
         for u in range(XS):
             last(b, u)
@@ -776,16 +824,34 @@
             at = g * group + u * width
             r.out[:, at : at + width] = r.acc[g, u].astype(BF16)
 
-    for guard, builds in started.items():
-
-        def drain(builds=builds):
-            for build in builds:
-                build().wait_send()
-
-        if guard is None:
-            drain()
-        else:
-            pl.when(guards[guard])(drain)
+    sent(r.wg.at[:2, : nz + 1], r.f_send)
+    sent(r.hidden.at[0], r.hx_send)
+    sent(r.s1, r.t1_send)
+    sent(r.s2, r.t2_send)
+    sent(r.s3, r.t3_send)
+    sent(r.s3x, r.t3x_send)
+    for build in (cross_c(c), cross_t(c), rows_c, mix_c, mix_y):
+        build().wait_send()
+
+    @pl.when(c == 0)
+    def _():
+        sent(r.wg.at[:, : CS * (nz - 1)], r.w_send)
+        near_c().wait_send()
+        near_t().wait_send()
+
+    @pl.when(c == 1)
+    def _():
+        sent(r.slab, r.h_send)
+        sent(r.normed.at[:3, :CS], r.nz_send)
+        sent(r.normed.at[:CS], r.ny_send)
+        sent(r.normed.at[: nz - 1, :CS], r.nd_send.at[0])
+        sent(r.normed.at[:CS], r.nd_send.at[1])
+        for build in (state_x(0), state_x(1), state_c):
+            build().wait_send()
+
+    @pl.when(jnp.logical_and(c == 1, z < nz - 1))
+    def _():
+        chain().wait_send()
 
 
 def fast_body(
@@ -863,22 +929,24 @@
         "acc": vmem((nz, XS, quarter, width), F32),
         "normed": vmem((nz, nt, quarter, model), BF16),
         "gated": vmem((nz // 2, 2 * rows, share), F32),
-        "hidden": vmem((nz * rows, share), BF16),
+        "hidden": vmem((XS, nz * rows, share), BF16),
         "keep": vmem((nz, XS, nt // CS, nz, quarter, width), F32),
         "s1": vmem((nz, XS, nt // CS, nz, quarter, width), BF16),
         "r1": vmem((nz, XS, nt // CS, nz, quarter, width), BF16),
         "s2": vmem((nz, XS, nz, quarter, width), BF16),
         "r2": vmem((nz, XS, nz, quarter, width), BF16),
-        "s3": vmem((nz, XS, nz, quarter, width), BF16),
-        "r3": vmem((nz, XS, nz, quarter, width), BF16),
+        "s3": vmem((nz + 2, nz - 1, quarter, width), BF16),
+        "r3": vmem((nz + 2, nz - 1, quarter, width), BF16),
+        "s3x": vmem((2, nz, quarter, width), BF16),
+        "r3x": vmem((2, nz, quarter, width), BF16),
         "in_sem": dma((len(operands),)),
         "own_sem": dma((3,)),
-        "h_send": dma((3,)),
+        "h_send": dma,
         "h_recv": dma((3,)),
-        "w_send": dma((CS, 3, nz)),
-        "w_recv": dma((3, nz)),
-        "f_send": dma((3, nz)),
-        "f_recv": dma((3, nz)),
+        "w_send": dma,
+        "w_recv": dma((3, nz - 1)),
+        "f_send": dma,
+        "f_recv": dma((4,)),
         "cx_send": dma((2,)),
         "cx_recv": dma((2, CS)),
         "cc_send": dma((2,)),
@@ -891,18 +959,22 @@
         "mix_recv": dma((2,)),
         "nc_send": dma,
         "nc_recv": dma,
-        "nz_send": dma((3, CS)),
+        "nz_send": dma,
         "nz_recv": dma((3, CS)),
-        "ny_send": dma((nz, CS)),
+        "ny_send": dma,
         "ny_recv": dma((nz, CS)),
-        "nd_send": dma((2, nz, CS)),
-        "nd_recv": dma((2, nz, CS)),
-        "t1_send": dma((nz, XS)),
+        "nd_send": dma((2,)),
+        "nd_recv": dma((2, nz)),
+        "t1_send": dma,
         "t1_recv": dma((nz, XS)),
-        "t2_send": dma((nz, XS)),
+        "t2_send": dma,
         "t2_recv": dma((nz, XS)),
-        "t3_send": dma((nz, XS, nz)),
-        "t3_recv": dma((nz, XS, nz)),
+        "t3_send": dma,
+        "t3_recv": dma((nz + 2,)),
+        "t3x_send": dma,
+        "t3x_recv": dma((2,)),
+        "hx_send": dma,
+        "hx_recv": dma((2,)),
     }
     names = list(operands) + ["out"] + list(scratch)
     return pl.pallas_call(

time: 81 us -> 78.5 us (0.969)
  Pallas kernels: 80.1 us -> 77.7 us
    pallas_call x1, Pallas kernels: 80.1 us -> 77.7 us  [fast_body(): pl.pallas_call(functools.partial(kernel, names, nz, nt), out_shape=pltpu....]
where the time goes in v3:
time: 78.5 us; the launch traced here: 78.4 us
  Pallas kernels  77.7 us (99%)
    pallas_call x1, Pallas kernels, fast_body(): pl.pallas_call(functools.partial(kernel, names, nz, nt), out_shape=pltpu....  77.7 us

profile of v3, /device:TPU:0, one launch (start us, length us, event | category | flops | bytes accessed | tf_op | source)
XLA Modules:
  0.0 78.4 jit_solution(892457879774020548)
XLA Ops:
  0.0 77.7 %shard_map.118 = bf16[32,2048]{1,0:T(8,128)(2,1)S(1)} custom-call(bf16[128,512]{1,0:T(8,128)(2,1)} %refs_0_.1, bf16[128,512]{1,0:T(8,128)(2,1)} %refs_1_.1, bf16[128,512]{1,0:T(8,128)(2,1)} %refs_2_.1, bf16[128,512]{1,0:T(8,128)(2,1)} %refs_3_.1, f32[4,128]{1,0:T(4,128)} %bitcast.4, f32[1,512]{1,0:T(1,128)} %bitcast.5, bf16[128,2048]{1,0:T(8,128)(2,1)} %refs_6_.1, ...), custom_call_target="tpu_custom_call" | custom-call | tf_op jit(solution)/shard_map/pallas_call | solution.py:980
  77.7 0.7 copy.14

commit v4 on v3

--- a/solution.py
+++ b/solution.py
@@ -274,7 +274,7 @@
     outer_head = ((0, 1), (1, 1))
     outer_tail = ((2, 1), (0, 2), (0, 3), (1, 2), (1, 3))
     inner_head = ((0, 3), (0, 1), (1, 3), (1, 1))
-    inner_tail = ((0, 2), (2, 1), (1, 2))
+    inner_tail = ((2,1),(0,2),(1,2))
 
     def send_weights(plan, which=range(CS)):
         for m, e in plan:
@@ -590,12 +590,13 @@
 
     @pl.when(c == 1)
     def _():
+        go(rows_z(0, 1))
+        go(rows_y(0, 1))
+        rows_c().wait_recv()
+        go(rows_z(0, 0))
         for j in (1, 0):
-            if j == 0:
-                rows_c().wait_recv()
-            for k in range(2):
-                go(rows_z(k, j))
-            go(rows_y(0, j))
+            go(rows_z(1, j))
+        go(rows_y(0, 0))
 
     @pl.when(c == 0)
     def _():
@@ -798,18 +799,18 @@
     got_weight(2, 3)
     compute(3, 0)
     third(0, 0)
+    second(3, 0)
     third(0, 1)
-    second(3, 0)
-    third(1, 0)
     got_weight(2, 2)
     compute(2, 0)
     other_hidden()
     compute(3, 1)
     compute(2, 1)
-    third(1, 1)
+    third(1, 0)
     second(2, 0)
     second(3, 1)
     second(2, 1)
+    third(1, 1)
     third(3, 0)
     third(2, 0)
     third(3, 1)

time: 78.5 us -> 78 us (level)
  no operation moved by 1% of the time
where the time goes in v4:
time: 78 us; the launch traced here: 77.8 us
  Pallas kernels  77.1 us (99%)
    pallas_call x1, Pallas kernels, fast_body(): pl.pallas_call(functools.partial(kernel, names, nz, nt), out_shape=pltpu....  77.1 us

profile of v4, /device:TPU:0, one launch (start us, length us, event | category | flops | bytes accessed | tf_op | source)
XLA Modules:
  0.0 77.8 jit_solution(14979891699437415044)
XLA Ops:
  0.0 77.1 %shard_map.118 = bf16[32,2048]{1,0:T(8,128)(2,1)S(1)} custom-call(bf16[128,512]{1,0:T(8,128)(2,1)} %refs_0_.1, bf16[128,512]{1,0:T(8,128)(2,1)} %refs_1_.1, bf16[128,512]{1,0:T(8,128)(2,1)} %refs_2_.1, bf16[128,512]{1,0:T(8,128)(2,1)} %refs_3_.1, f32[4,128]{1,0:T(4,128)} %bitcast.4, f32[1,512]{1,0:T(1,128)} %bitcast.5, bf16[128,2048]{1,0:T(8,128)(2,1)} %refs_6_.1, ...), custom_call_target="tpu_custom_call" | custom-call | tf_op jit(solution)/shard_map/pallas_call | solution.py:981
  77.2 0.7 copy.14

commit v5 on v4

--- a/solution.py
+++ b/solution.py
@@ -253,74 +253,6 @@
         take_own(m)
     loads["dw"].wait()
     take_own(2)
-    pl.semaphore_wait(barrier, len(peers))
-
-    def hand(m):
-        return lambda: remote(
-            r.slab.at[m], r.partner.at[m], r.h_send, r.h_recv.at[m], c_peer
-        )
-
-    def weight(m, e, k):
-        source = r.partner if k else r.slab
-        return lambda: remote(
-            piece(source, m, zat[e]),
-            slot(m, z),
-            r.w_send,
-            r.w_recv.at[m, e - 1],
-            dev(zat[e], x, y, k),
-        )
-
-    outer = jnp.logical_or(z == 0, z == nz - 1)
-    outer_head = ((0, 1), (1, 1))
-    outer_tail = ((2, 1), (0, 2), (0, 3), (1, 2), (1, 3))
-    inner_head = ((0, 3), (0, 1), (1, 3), (1, 1))
-    inner_tail = ((2,1),(0,2),(1,2))
-
-    def send_weights(plan, which=range(CS)):
-        for m, e in plan:
-            for k in which:
-                weight(m, e, k)().start()
-
-    def got_weight(m, e):
-        weight(m, e, 0)().wait_recv()
-
-    def forward(m, e):
-        at = slot(m, zat[e])
-        source = piece(r.slab, m, z) if e == 0 else at
-        recv = r.f_recv.at[2 + e] if m == 2 else r.f_recv.at[m]
-        return lambda: remote(source, at, r.f_send, recv, x_peer)
-
-    def pass_on(m, e):
-        if e:
-            got_weight(m, e)
-        go(forward(m, e))
-
-    def pass_if(when, pieces):
-        @pl.when(when)
-        def _():
-            for m, e in pieces:
-                got_weight(m, e)
-                forward(m, e)().start()
-
-    near = ((0, 1), (1, 1))
-
-    def got_forwards(m):
-        view = r.wg.at[m, :nz]
-        remote(view, view, r.f_send, r.f_recv.at[m], x_peer).wait_recv()
-
-    @pl.when(c == 1)
-    def _():
-        for m in range(3):
-            go(hand(m))
-
-    @pl.when(jnp.logical_and(c == 0, outer))
-    def _():
-        send_weights(outer_head, (0,))
-
-    @pl.when(jnp.logical_and(c == 0, jnp.logical_not(outer)))
-    def _():
-        send_weights(inner_head, (0,))
-
     for name in ("ld", "q", "k", "v"):
         loads[name].wait()
     ti = lax.broadcasted_iota(jnp.int32, (rows, rows), 0)
@@ -361,6 +293,74 @@
         r.t_out[h] = jnp.broadcast_to(jnp.exp(last), r.t_out.shape[1:])
         r.qrot[:, cols] = qb
         r.cumx[:, cols] = jnp.exp(cum)
+
+    pl.semaphore_wait(barrier, len(peers))
+
+    def hand(m):
+        return lambda: remote(
+            r.slab.at[m], r.partner.at[m], r.h_send, r.h_recv.at[m], c_peer
+        )
+
+    def weight(m, e, k):
+        source = r.partner if k else r.slab
+        return lambda: remote(
+            piece(source, m, zat[e]),
+            slot(m, z),
+            r.w_send,
+            r.w_recv.at[m, e - 1],
+            dev(zat[e], x, y, k),
+        )
+
+    outer = jnp.logical_or(z == 0, z == nz - 1)
+    outer_head = ((0, 1), (1, 1))
+    outer_tail = ((2, 1), (0, 2), (0, 3), (1, 2), (1, 3))
+    inner_head = ((0, 3), (0, 1), (1, 3), (1, 1))
+    inner_tail = ((2,1),(0,2),(1,2))
+
+    def send_weights(plan, which=range(CS)):
+        for m, e in plan:
+            for k in which:
+                weight(m, e, k)().start()
+
+    def got_weight(m, e):
+        weight(m, e, 0)().wait_recv()
+
+    def forward(m, e):
+        at = slot(m, zat[e])
+        source = piece(r.slab, m, z) if e == 0 else at
+        recv = r.f_recv.at[2 + e] if m == 2 else r.f_recv.at[m]
+        return lambda: remote(source, at, r.f_send, recv, x_peer)
+
+    def pass_on(m, e):
+        if e:
+            got_weight(m, e)
+        go(forward(m, e))
+
+    def pass_if(when, pieces):
+        @pl.when(when)
+        def _():
+            for m, e in pieces:
+                got_weight(m, e)
+                forward(m, e)().start()
+
+    near = ((0, 1), (1, 1))
+
+    def got_forwards(m):
+        view = r.wg.at[m, :nz]
+        remote(view, view, r.f_send, r.f_recv.at[m], x_peer).wait_recv()
+
+    @pl.when(c == 1)
+    def _():
+        for m in range(3):
+            go(hand(m))
+
+    @pl.when(jnp.logical_and(c == 0, outer))
+    def _():
+        send_weights(outer_head, (0,))
+
+    @pl.when(jnp.logical_and(c == 0, jnp.logical_not(outer)))
+    def _():
+        send_weights(inner_head, (0,))
 
     my_h, its_h = pl.ds(x * hh, hh), pl.ds((1 - x) * hh, hh)
     x_one, c_one = dev(z, 1 - x, y, 1), dev(z, x, y, 1)

time: 78 us -> 77.7 us (level)
  no operation moved by 1% of the time
where the time goes in v5:
time: 77.7 us; the launch traced here: 77.6 us
  Pallas kernels  76.9 us (99%)
    pallas_call x1, Pallas kernels, fast_body(): pl.pallas_call(functools.partial(kernel, names, nz, nt), out_shape=pltpu....  76.9 us

profile of v5, /device:TPU:0, one launch (start us, length us, event | category | flops | bytes accessed | tf_op | source)
XLA Modules:
  0.0 77.6 jit_solution(6446934667368229848)
XLA Ops:
  0.0 76.9 %shard_map.118 = bf16[32,2048]{1,0:T(8,128)(2,1)S(1)} custom-call(bf16[128,512]{1,0:T(8,128)(2,1)} %refs_0_.1, bf16[128,512]{1,0:T(8,128)(2,1)} %refs_1_.1, bf16[128,512]{1,0:T(8,128)(2,1)} %refs_2_.1, bf16[128,512]{1,0:T(8,128)(2,1)} %refs_3_.1, f32[4,128]{1,0:T(4,128)} %bitcast.4, f32[1,512]{1,0:T(1,128)} %bitcast.5, bf16[128,2048]{1,0:T(8,128)(2,1)} %refs_6_.1, ...), custom_call_target="tpu_custom_call" | custom-call | tf_op jit(solution)/shard_map/pallas_call | solution.py:981
  76.9 0.7 copy.14
